TPU v7x, 32 devices: a whole 2x2x4 slice. The times are simulated.
32 devices in a mesh: sp: 4 (over y, x), tp: 8 (over z, core).
Axes of the slice: x: 2, y: 2, z: 4, core: 2. Of those that a mesh axis runs over, the one named last changes fastest.
Arguments:
- prompt: bfloat16 [2, 8, 2, 4, 128, 2048], P(None, 'tp', None, 'sp'), may hold values from -60 to 60
- new_token: bfloat16 [2, 2048], replicated, may hold values from -20 to 20
- query_proj_matrix: bfloat16 [2048, 1024], P(None, 'tp'), may hold values from -1 to 1
- key_weight: bfloat16 [2048, 1024], P(None, 'tp'), may hold values from -1 to 1
- value_weight: bfloat16 [2048, 1024], P(None, 'tp'), may hold values from -0.125 to 0.125
- map_balance: float32 [8], replicated, may hold values from 0.3 to 0.8
- head_gain: float32 [128], replicated, may hold values from 0.1 to 1.9
Outputs:
- key_cache: bfloat16 [4, 8, 512, 1024], P('sp', 'tp')
- value_cache: bfloat16 [4, 8, 512, 1024], P('sp', 'tp')
- read: float32 [2, 1024], replicated
All inputs are finite; a program needn't handle non-finite values.
Results may differ from a plain program's by a relative error of at most 0.004.
The roundings to bfloat16 on the way count: a program that leaves them out, or rounds other values in their place, can miss the bound.
Values may be sent and summed in bfloat16 or wider, within the bound.
A program may use at most 64 MiB of HBM per device.

v0:
```python
import functools

import jax
import jax.numpy as jnp
from jax import lax
from jax.experimental import pallas as pl
from jax.experimental.pallas import tpu as pltpu
from jax.sharding import PartitionSpec as P

HEADS = 8
MAP_HEAD_SIZE = 64
VD = 128


norm_eps = 1e-06
far_below = -1e30


def joined(part, axis, combine):
    gathered = jax.tree.map(lambda a: lax.all_gather(a, axis), part)

    def take(source):
        return jax.tree.map(lambda a: lax.dynamic_index_in_dim(a, source, 0, False), gathered)

    return lax.fori_loop(
        1, lax.axis_size(axis), lambda source, state: combine(state, take(source)), take(0)
    )


def fill_cols(source, w_piece):
    product = jnp.dot(source, w_piece, preferred_element_type=jnp.float32).astype(jnp.bfloat16)
    return product


def local_new(new_token, query_proj_matrix, key_weight, value_weight):
    return (
        jnp.dot(new_token, query_proj_matrix, preferred_element_type=jnp.float32).astype(
            jnp.bfloat16
        ),
        jnp.dot(new_token, key_weight, preferred_element_type=jnp.float32).astype(jnp.bfloat16),
        jnp.dot(new_token, value_weight, preferred_element_type=jnp.float32).astype(jnp.bfloat16),
    )


def partial_read(query_matrix_rows, key_rows, value_rows):
    logit_scores = jnp.einsum(
        "bhmd,bjhmd->bhmj", query_matrix_rows, key_rows, preferred_element_type=jnp.float32
    ) * MAP_HEAD_SIZE ** (-0.5)
    peak = jnp.max(logit_scores, axis=-1)
    weights_exp = jnp.exp(logit_scores - peak[..., None])
    totals = jnp.sum(weights_exp, axis=-1)
    weighted = jnp.einsum("bhmj,bjhe->bhme", weights_exp, value_rows.astype(jnp.float32))
    return (peak, totals, weighted)


def combine(first, second):
    peak_a, totals_a, weighted_a = first
    peak_b, totals_b, weighted_b = second
    peak = jnp.maximum(peak_a, peak_b)
    factor_a = jnp.exp(peak_a - peak)
    factor_b = jnp.exp(peak_b - peak)
    return (
        peak,
        totals_a * factor_a + totals_b * factor_b,
        weighted_a * factor_a[..., None] + weighted_b * factor_b[..., None],
    )


def shards(prompt, new_token, query_proj_matrix, key_weight, value_weight, map_balance, head_gain):
    seq_count, _, span_count, _, piece_rows, model_width = prompt.shape
    token_rows = prompt.reshape(seq_count * span_count * piece_rows, model_width)
    tp_count = lax.axis_size("tp")
    key_width = key_weight.shape[1] * tp_count
    value_width = value_weight.shape[1] * tp_count
    key_piece = lax.all_gather(key_weight, "tp", axis=1, tiled=True)
    value_piece = lax.all_gather(value_weight, "tp", axis=1, tiled=True)
    key_rows = fill_cols(token_rows, key_piece)
    value_rows = fill_cols(token_rows, value_piece)
    own_columns = local_new(new_token, query_proj_matrix, key_weight, value_weight)
    queries, new_keys, new_values = (
        lax.all_gather(own_columns[0], "tp", axis=1, tiled=True),
        lax.all_gather(own_columns[1], "tp", axis=1, tiled=True),
        lax.all_gather(own_columns[2], "tp", axis=1, tiled=True),
    )
    slot_count = seq_count * span_count
    cached_keys, cached_values = (
        lax.all_to_all(
            key_rows.reshape(slot_count, piece_rows, key_width),
            "sp",
            split_axis=0,
            concat_axis=1,
            tiled=True,
        ),
        lax.all_to_all(
            value_rows.reshape(slot_count, piece_rows, value_width),
            "sp",
            split_axis=0,
            concat_axis=1,
            tiled=True,
        ),
    )
    block_rows = cached_keys.shape[1]
    key_cache = cached_keys.reshape(1, 1, block_rows, key_width)
    value_cache = cached_values.reshape(1, 1, block_rows, value_width)
    all_queries = queries.reshape(seq_count, HEADS, 2, MAP_HEAD_SIZE)
    own_seq = lax.axis_index("sp") // span_count
    own_query = lax.dynamic_slice_in_dim(all_queries, own_seq, 1, 0)
    peak, totals, weighted = partial_read(
        own_query,
        cached_keys.reshape(1, block_rows, HEADS, 2, MAP_HEAD_SIZE),
        cached_values.reshape(1, block_rows, HEADS, VD),
    )
    chosen = jnp.arange(seq_count) == own_seq
    chosen_rows = chosen[:, None, None]
    spread = (
        jnp.where(chosen_rows, peak, far_below),
        jnp.where(chosen_rows, totals, 0.0),
        jnp.where(chosen_rows[..., None], weighted, 0.0),
    )
    merged = joined(spread, ("sp", "tp"), combine)
    own_keys = new_keys.reshape(seq_count, HEADS, 2, MAP_HEAD_SIZE)
    own_score = jnp.einsum(
        "bhmd,bhmd->bhm", all_queries, own_keys, preferred_element_type=jnp.float32
    ) * MAP_HEAD_SIZE ** (-0.5)
    own_values = new_values.astype(jnp.float32).reshape(seq_count, HEADS, VD)
    own_weighted = jnp.broadcast_to(own_values[:, :, None, :], (seq_count, HEADS, 2, VD))
    own_state = (own_score, jnp.ones_like(own_score), own_weighted)
    _, totals, weighted = combine(merged, own_state)
    heads_out = weighted / totals[..., None]
    blended = heads_out[:, :, 0] - map_balance[None, :, None] * heads_out[:, :, 1]
    normed = (
        blended
        * lax.rsqrt(jnp.mean(blended * blended, axis=-1, keepdims=True) + norm_eps)
        * head_gain
    )
    return (key_cache, value_cache, normed.reshape(seq_count, HEADS * VD))


MESH = pl.DeviceIdType.MESH
CORES = 2
PIECES = 2


def merged_states(states):
    half = VD // 2
    peaks = [a[:, VD : VD + 1] for a in states]
    totals = [a[:, VD + half : VD + half + 1] for a in states]
    peak = functools.reduce(jnp.maximum, peaks)
    factors = [jnp.exp(p - peak) for p in peaks]
    total = functools.reduce(jnp.add, [t * f for t, f in zip(totals, factors)])
    weighted = functools.reduce(jnp.add, [a[:, :VD] * f for a, f in zip(states, factors)])
    return weighted, peak, total


def packed_state(weighted, peak, total):
    lane = lax.broadcasted_iota(jnp.int32, weighted.shape, 1)
    tail = jnp.where(lane < VD // 2, peak, total)
    return jnp.concatenate([weighted, tail], axis=1)


def step_kernel(
    dims,
    prompt, token, wq_hbm, wk_hbm, wv_hbm, balance, gain,
    kout, vout, read,
    xbuf, wbuf, wq, qbuf, own, stbuf, finbuf,
    loc, pr_send, pr_recv, line_send, prim_recv, sib_send, sib_recv, xy_send, sec_recv,
    pk_send, pk_recv, st_send, st_recv, fin_send, fin_recv,
):
    sp_count, tp_count, seq_count = dims
    depth = wbuf.shape[2]
    cols = wbuf.shape[3] // CORES
    chips = tp_count // CORES
    s = lax.axis_index("sp")
    t = lax.axis_index("tp")
    z = t // CORES
    c = t % CORES
    sib = z * CORES + (1 - c)
    xs = s + 1 - 2 * (s % 2)
    ys = (s + 2) % 4
    prim = (s + s // 2) % 2
    sec = 1 - prim
    lanes = pl.ds(pl.multiple_of(c * cols, cols), cols)
    step = depth // PIECES
    half = step // 2

    loads = [
        pltpu.make_async_copy(wk_hbm, wbuf.at[0, z, :, lanes], loc.at[0]),
        pltpu.make_async_copy(wv_hbm, wbuf.at[1, z, :, lanes], loc.at[1]),
        pltpu.make_async_copy(wq_hbm, wq, loc.at[2]),
        pltpu.make_async_copy(prompt.at[s], xbuf.at[s], loc.at[3]),
    ]
    for a in loads:
        a.start()

    barrier = pltpu.get_barrier_semaphore()
    for d in range(1, sp_count):
        pl.semaphore_signal(barrier, inc=1, device_id=((s + d) % sp_count, t), device_id_type=MESH)
    for d in range(1, tp_count):
        pl.semaphore_signal(barrier, inc=1, device_id=(s, (t + d) % tp_count), device_id_type=MESH)
    pl.semaphore_wait(barrier, sp_count + tp_count - 2)

    def remote(src, dst, send, recv, dev):
        return pltpu.make_async_remote_copy(
            src_ref=src, dst_ref=dst, send_sem=send, recv_sem=recv, device_id=dev, device_id_type=MESH
        )

    def block(m, zz):
        return wbuf.at[m, zz, :, lanes]

    def piece_of(m, zz, p):
        return wbuf.at[m, zz, pl.ds(p * step, step), lanes]

    def part(m, zz, p, h):
        return wbuf.at[m, zz, pl.ds(p * step + h * half, half), lanes]

    sends = []

    def go(copy):
        copy.start()
        sends.append(copy)

    loads[0].wait()
    loads[1].wait()

    def line(direction, zz, p):
        return remote(
            piece_of(prim, zz, p), piece_of(prim, zz, p),
            line_send.at[(direction + 1) // 2, zz, p], prim_recv.at[zz, p],
            (s, t + direction * CORES),
        )

    def has_next(direction):
        return (z > 0) if direction < 0 else (z < chips - 1)

    for direction in (-1, 1):
        @pl.when(has_next(direction))
        def _(direction=direction):
            for p in range(PIECES):
                line(direction, z, p).start()

    for d in (1, 2, 3):
        p = xs if d == 1 else ys if d == 2 else 3 - s
        go(remote(prompt.at[p], xbuf.at[s], pr_send.at[d], pr_recv.at[s], (p, t)))
    for m in range(2):
        go(remote(block(m, z), block(m, z), sib_send.at[m, z, 0], sib_recv.at[m, z, 0], (s, sib)))

    loads[2].wait()
    rows = token[...]
    me_q = jnp.dot(rows, wq[...], preferred_element_type=jnp.float32)
    me_k = jnp.dot(rows, wbuf[0, z, :, lanes], preferred_element_type=jnp.float32)
    me_v = jnp.dot(rows, wbuf[1, z, :, lanes], preferred_element_type=jnp.float32)
    for i, value in enumerate((me_q, me_k, me_v)):
        value = value.astype(jnp.bfloat16).astype(jnp.float32)
        qbuf[t, i * seq_count : (i + 1) * seq_count, :] = value[:seq_count]
    for d in range(1, tp_count):
        go(remote(qbuf.at[t], qbuf.at[t], pk_send.at[d], pk_recv.at[t], (s, (t + d) % tp_count)))

    near = jnp.minimum(z, chips - 1 - z)

    def source(j):
        paired = j <= 2 * near
        dist = jnp.where(paired, (j + 1) // 2, j - near)
        from_left = jnp.where(paired, j % 2 == 1, z > near)
        return jnp.where(from_left, z - dist, z + dist), from_left

    sources = [source(j) for j in range(1, chips)]

    def forwards(from_left):
        return (
            jnp.logical_and(from_left, z < chips - 1),
            jnp.logical_and(jnp.logical_not(from_left), z > 0),
        )

    def primary_copies(j, p):
        zz, _ = sources[j]
        copies = []
        for h, to in enumerate((xs, ys)):
            view = part(prim, zz, p, h)
            copies.append(remote(view, view, xy_send.at[h, zz, p], sec_recv.at[h, zz, p], (to, t)))
        view = piece_of(prim, zz, p)
        copies.append(remote(view, view, sib_send.at[0, zz, p], sib_recv.at[0, zz, p], (s, sib)))
        return copies

    def arrive_primary(j, p):
        zz, from_left = sources[j]
        view = piece_of(prim, zz, p)
        remote(view, view, line_send.at[0, zz, p], prim_recv.at[zz, p], (s, t)).wait_recv()
        for on, direction in zip(forwards(from_left), (1, -1)):
            pl.when(on)(lambda direction=direction: line(direction, zz, p).start())
        for copy in primary_copies(j, p):
            copy.start()

    def arrive_secondary(j):
        zz, _ = sources[j]
        for p in range(PIECES):
            for h in range(2):
                view = part(sec, zz, p, h)
                remote(view, view, xy_send.at[h, zz, p], sec_recv.at[h, zz, p], (s, t)).wait_recv()
                i = 2 * p + h
                go(remote(view, view, sib_send.at[1, zz, i], sib_recv.at[1, zz, i], (s, sib)))

    sib_lanes = pl.ds(pl.multiple_of((1 - c) * cols, cols), cols)

    def wait_sibling(m, slot, zz, parts):
        size = depth // parts
        for i in range(parts):
            view = wbuf.at[m, zz, pl.ds(i * size, size), sib_lanes]
            remote(view, view, sib_send.at[slot, zz, i], sib_recv.at[slot, zz, i], (s, t)).wait_recv()

    def multiply(m, zz):
        weights = wbuf.at[m, zz]
        columns = pl.ds(pl.multiple_of(zz * CORES * cols, CORES * cols), CORES * cols)

        def piece(i, _):
            product = jnp.dot(
                xbuf[pl.ds(2 * i, 2)].reshape(-1, depth), weights[...], preferred_element_type=jnp.float32
            ).astype(jnp.bfloat16)
            at = pl.ds(pl.multiple_of(i * product.shape[0], product.shape[0]), product.shape[0])

            def put(out):
                out[at, columns] = product

            if isinstance(m, int):
                put((kout, vout)[m])
            else:
                pl.when(m == 0)(lambda: put(kout))
                pl.when(m == 1)(lambda: put(vout))
            return 0

        lax.fori_loop(0, sp_count // 2, piece, 0)

    def multiply_primary(j):
        zz, _ = sources[j]
        wait_sibling(prim, 0, zz, PIECES)
        multiply(prim, zz)

    def multiply_secondary(j):
        zz, _ = sources[j]
        wait_sibling(sec, 1, zz, 2 * PIECES)
        multiply(sec, zz)

    last = chips - 1
    for j in range(min(2, last)):
        for p in range(PIECES):
            arrive_primary(j, p)
    inside = near > 0

    @pl.when(inside)
    def _():
        for j in range(2, last):
            for p in range(PIECES):
                arrive_primary(j, p)

    for d in range(1, tp_count):
        i = (t + d) % tp_count
        remote(qbuf.at[i], qbuf.at[i], pk_send.at[d], pk_recv.at[i], (s, t)).wait_recv()
    new = jnp.concatenate([qbuf[i] for i in range(tp_count)], axis=1)
    row = lax.broadcasted_iota(jnp.int32, (2 * HEADS, new.shape[1]), 0)
    lane = lax.broadcasted_iota(jnp.int32, (2 * HEADS, new.shape[1]), 1)
    own_lane = lane // MAP_HEAD_SIZE == (row % HEADS) * 2 + row // HEADS
    scale = MAP_HEAD_SIZE ** (-0.5)
    short_row = lax.broadcasted_iota(jnp.int32, (2 * HEADS, VD), 0) % HEADS

    def by_head(wide):
        return functools.reduce(
            jnp.add,
            [jnp.where(short_row == h, wide[:, h * VD : (h + 1) * VD], 0.0) for h in range(HEADS)],
        )

    own_seq = s // (sp_count // seq_count)
    query = jnp.zeros((2 * HEADS, new.shape[1]), jnp.float32)
    for b in range(seq_count):
        q_b = jnp.broadcast_to(new[b : b + 1], query.shape)
        k_b = jnp.broadcast_to(new[seq_count + b : seq_count + b + 1], query.shape)
        v_b = jnp.broadcast_to(new[2 * seq_count + b : 2 * seq_count + b + 1], query.shape)
        score = jnp.sum(jnp.where(own_lane, q_b * k_b, 0.0), axis=1, keepdims=True) * scale
        own[b] = packed_state(by_head(v_b), score, jnp.ones_like(score))
        query = jnp.where(own_seq == b, q_b, query)
    query = jnp.where(own_lane, query, 0.0).astype(jnp.bfloat16)

    loads[3].wait()
    for d, p in ((1, xs), (2, ys), (3, 3 - s)):
        remote(xbuf.at[p], xbuf.at[p], pr_send.at[d], pr_recv.at[p], (s, t)).wait_recv()
    for m in range(2):
        wait_sibling(m, m, z, 1)
        multiply(m, z)
    multiply_primary(0)
    for j in range(1, last):
        arrive_secondary(j - 1)
        later = range(PIECES) if j + 1 < last else ()
        for p in later:
            pl.when(jnp.logical_not(inside))(lambda: arrive_primary(j + 1, p))
            if p == 0:
                multiply_primary(j)
        if j + 1 == last and last < 3:
            multiply_primary(j)
        multiply_secondary(j - 1)
    if last > 2:
        multiply_primary(last - 1)
    arrive_secondary(last - 1)
    multiply_secondary(last - 1)

    scores = lax.dot_general(
        query, kout[...], (((1,), (1,)), ((), ())), preferred_element_type=jnp.float32
    ) * scale
    peak = jnp.max(scores, axis=1, keepdims=True)
    raised = jnp.exp(scores - peak)
    total = jnp.sum(raised, axis=1, keepdims=True)
    high = raised.astype(jnp.bfloat16)
    low = (raised - high.astype(jnp.float32)).astype(jnp.bfloat16)
    wide = jnp.dot(high, vout[...], preferred_element_type=jnp.float32)
    wide = wide + jnp.dot(low, vout[...], preferred_element_type=jnp.float32)
    stbuf[t] = packed_state(by_head(wide), peak, total)
    for d in range(1, tp_count):
        go(remote(stbuf.at[t], stbuf.at[t], st_send.at[d], st_recv.at[t], (s, (t + d) % tp_count)))
    for d in range(1, tp_count):
        i = (t + d) % tp_count
        remote(stbuf.at[i], stbuf.at[i], st_send.at[d], st_recv.at[i], (s, t)).wait_recv()
    finbuf[s] = packed_state(*merged_states([stbuf[i] for i in range(tp_count)]))
    for d in range(1, sp_count):
        go(remote(finbuf.at[s], finbuf.at[s], fin_send.at[d], fin_recv.at[s], ((s + d) % sp_count, t)))
    for d in range(1, sp_count):
        i = (s + d) % sp_count
        remote(finbuf.at[i], finbuf.at[i], fin_send.at[d], fin_recv.at[i], (s, t)).wait_recv()
    spans = sp_count // seq_count
    square = (HEADS, HEADS)
    diagonal = lax.broadcasted_iota(jnp.int32, square, 0) == lax.broadcasted_iota(jnp.int32, square, 1)
    second = jnp.sum(jnp.where(diagonal, balance[...], 0.0), axis=1, keepdims=True)
    for b in range(seq_count):
        weighted, _, total = merged_states([finbuf[b * spans + i] for i in range(spans)] + [own[b]])
        heads_out = weighted / total
        blended = heads_out[:HEADS] - second * heads_out[HEADS:]
        normed = (
            blended * lax.rsqrt(jnp.mean(blended * blended, axis=1, keepdims=True) + norm_eps) * gain[...]
        )
        for h in range(HEADS):
            read[b : b + 1, h * VD : (h + 1) * VD] = normed[h : h + 1]

    for p in range(PIECES):
        for direction in (-1, 1):
            pl.when(has_next(direction))(
                lambda direction=direction, p=p: line(direction, z, p).wait_send()
            )
        for zz, from_left in sources:
            for on, direction in zip(forwards(from_left), (1, -1)):
                pl.when(on)(
                    lambda direction=direction, zz=zz, p=p: line(direction, zz, p).wait_send()
                )
    for j in range(last):
        for p in range(PIECES):
            sends.extend(primary_copies(j, p))
    for copy in sends:
        copy.wait_send()


def fused(prompt, new_token, query_proj_matrix, key_weight, value_weight, map_balance, head_gain):
    seq_count, _, span_count, _, piece_rows, width = prompt.shape
    sp_count, tp_count = lax.axis_size("sp"), lax.axis_size("tp")
    cols = key_weight.shape[1]
    slots = seq_count * span_count
    chips = tp_count // CORES
    key_width = cols * tp_count
    block_rows = sp_count * piece_rows
    any_space = pl.BlockSpec(memory_space=pltpu.HBM)
    vmem = pl.BlockSpec(memory_space=pltpu.VMEM)
    dma = pltpu.SemaphoreType.DMA
    keys, values, read = pl.pallas_call(
        functools.partial(step_kernel, (sp_count, tp_count, seq_count)),
        out_shape=[
            pltpu.VMEM((block_rows, key_width), jnp.bfloat16),
            pltpu.VMEM((block_rows, key_width), jnp.bfloat16),
            pltpu.VMEM((seq_count, HEADS * VD), jnp.float32),
        ],
        in_specs=[any_space, vmem, any_space, any_space, any_space, vmem, vmem],
        out_specs=[vmem, vmem, vmem],
        scratch_shapes=[
            pltpu.VMEM((sp_count, piece_rows, width), jnp.bfloat16),
            pltpu.VMEM((2, chips, width, CORES * cols), jnp.bfloat16),
            pltpu.VMEM((width, cols), jnp.bfloat16),
            pltpu.VMEM((tp_count, 8, cols), jnp.float32),
            pltpu.VMEM((seq_count, 2 * HEADS, 2 * VD), jnp.float32),
            pltpu.VMEM((tp_count, 2 * HEADS, 2 * VD), jnp.float32),
            pltpu.VMEM((sp_count, 2 * HEADS, 2 * VD), jnp.float32),
            dma((4,)), dma((4,)), dma((sp_count,)), dma((2, chips, PIECES)), dma((chips, PIECES)),
            dma((2, chips, 2 * PIECES)), dma((2, chips, 2 * PIECES)),
            dma((2, chips, PIECES)), dma((2, chips, PIECES)),
            dma((tp_count,)), dma((tp_count,)), dma((tp_count,)), dma((tp_count,)),
            dma((sp_count,)), dma((sp_count,)),
        ],
        compiler_params=pltpu.CompilerParams(
            collective_id=0, has_side_effects=True, vmem_limit_bytes=61 * 1024 * 1024 + 800 * 1024
        ),
    )(
        prompt.reshape(slots, piece_rows, width),
        new_token, query_proj_matrix, key_weight, value_weight,
        map_balance[None, :], head_gain[None, :],
    )
    shape = (1, 1, block_rows, key_width)
    return keys.reshape(shape), values.reshape(shape), read


def fits(mesh, key_weight, value_weight, prompt):
    tp_count, sp_count = mesh.shape["tp"], mesh.shape["sp"]
    seq_count, _, span_count = prompt.shape[:3]
    cols = key_weight.shape[1] // tp_count
    return (
        sp_count == 4
        and seq_count * span_count == sp_count
        and tp_count % CORES == 0
        and tp_count > CORES
        and cols % VD == 0
        and 3 * seq_count <= 8
        and key_weight.shape == value_weight.shape
    )


def solution(mesh):
    in_specs = (
        P(None, "tp", None, "sp", None, None),
        P(),
        P(None, "tp"),
        P(None, "tp"),
        P(None, "tp"),
        P(),
        P(),
    )
    out_specs = (P("sp", "tp", None, None), P("sp", "tp", None, None), P())

    def step(prompt, new_token, query_proj_matrix, key_weight, value_weight, map_balance, head_gain):
        body = fused if fits(mesh, key_weight, value_weight, prompt) else shards
        mapped = jax.shard_map(
            body, mesh=mesh, in_specs=in_specs, out_specs=out_specs, check_vma=False
        )
        return mapped(
            prompt, new_token, query_proj_matrix, key_weight, value_weight, map_balance, head_gain
        )

    return step
```

profile of v0, /device:TPU:0, one launch (start us, length us, event | category | flops | bytes accessed | tf_op | source)
XLA Modules:
  0.0 62.8 jit_solution(2811238797249538354)
XLA Ops:
  0.6 59.6 %shard_map.94 = (bf16[512,1024]{1,0:T(8,128)(2,1)S(1)}, bf16[512,1024]{1,0:T(8,128)(2,1)S(1)}, f32[2,1024]{1,0:T(2,128)S(1)}) custom-call(bf16[4,128,2048]{2,1,0:T(8,128)(2,1)} %bitcast.7, bf16[2,2048]{1,0:T(2,128)(2,1)} %token_.1, bf16[2048,128]{1,0:T(8,128)(2,1)} %wq_hbm.1, bf16[2048,128]{1,0:T(8,128)(2,1)} %wk_hbm.1, bf16[2048,128]{1,0:T(8,128)(2,1)} %wv_hbm.1, ...), custom_call_target="tpu_custom_call" | custom-call | tf_op jit(solution)/shard_map/pallas_call | solution.py:467
  60.2 1.0 %copy.13 = bf16[1,1,512,1024]{3,2,1,0:T(8,128)(2,1)} copy(bf16[1,1,512,1024]{3,2,1,0:T(8,128)(2,1)S(1)} %bitcast.6) | data formatting | bytes 2097152
  61.2 1.0 %copy.14 = bf16[1,1,512,1024]{3,2,1,0:T(8,128)(2,1)} copy(bf16[1,1,512,1024]{3,2,1,0:T(8,128)(2,1)S(1)} %bitcast.5) | data formatting | bytes 2097152
  62.2 0.6 copy.15
where the time goes:
time: 62.9 us; the launch traced here: 62.8 us
  Pallas kernels  59.6 us (95%)
  local copies, waits for them, and re-layouts  2.54 us (4%)
  between operations  0.64 us (1%)
    pallas_call x1, Pallas kernels, fused(): pl.pallas_call(functools.partial(step_kernel, (sp_count, tp_count, seq_co...  59.6 us
    unnamed x3, local copies, waits for them, and re-layouts  2.54 us

commit v1 on v0

v1 whole, which is shorter than its diff:
```python
import functools

import jax
import jax.numpy as jnp
from jax import lax
from jax.experimental import pallas as pl
from jax.experimental.pallas import tpu as pltpu
from jax.sharding import PartitionSpec as P

HEADS = 8
MAP_HEAD_SIZE = 64
VD = 128


norm_eps = 1e-06
far_below = -1e30


def joined(part, axis, combine):
    gathered = jax.tree.map(lambda a: lax.all_gather(a, axis), part)

    def take(source):
        return jax.tree.map(lambda a: lax.dynamic_index_in_dim(a, source, 0, False), gathered)

    return lax.fori_loop(
        1, lax.axis_size(axis), lambda source, state: combine(state, take(source)), take(0)
    )


def fill_cols(source, w_piece):
    product = jnp.dot(source, w_piece, preferred_element_type=jnp.float32).astype(jnp.bfloat16)
    return product


def local_new(new_token, query_proj_matrix, key_weight, value_weight):
    return (
        jnp.dot(new_token, query_proj_matrix, preferred_element_type=jnp.float32).astype(
            jnp.bfloat16
        ),
        jnp.dot(new_token, key_weight, preferred_element_type=jnp.float32).astype(jnp.bfloat16),
        jnp.dot(new_token, value_weight, preferred_element_type=jnp.float32).astype(jnp.bfloat16),
    )


def partial_read(query_matrix_rows, key_rows, value_rows):
    logit_scores = jnp.einsum(
        "bhmd,bjhmd->bhmj", query_matrix_rows, key_rows, preferred_element_type=jnp.float32
    ) * MAP_HEAD_SIZE ** (-0.5)
    peak = jnp.max(logit_scores, axis=-1)
    weights_exp = jnp.exp(logit_scores - peak[..., None])
    totals = jnp.sum(weights_exp, axis=-1)
    weighted = jnp.einsum("bhmj,bjhe->bhme", weights_exp, value_rows.astype(jnp.float32))
    return (peak, totals, weighted)


def combine(first, second):
    peak_a, totals_a, weighted_a = first
    peak_b, totals_b, weighted_b = second
    peak = jnp.maximum(peak_a, peak_b)
    factor_a = jnp.exp(peak_a - peak)
    factor_b = jnp.exp(peak_b - peak)
    return (
        peak,
        totals_a * factor_a + totals_b * factor_b,
        weighted_a * factor_a[..., None] + weighted_b * factor_b[..., None],
    )


def shards(prompt, new_token, query_proj_matrix, key_weight, value_weight, map_balance, head_gain):
    seq_count, _, span_count, _, piece_rows, model_width = prompt.shape
    token_rows = prompt.reshape(seq_count * span_count * piece_rows, model_width)
    tp_count = lax.axis_size("tp")
    key_width = key_weight.shape[1] * tp_count
    value_width = value_weight.shape[1] * tp_count
    key_piece = lax.all_gather(key_weight, "tp", axis=1, tiled=True)
    value_piece = lax.all_gather(value_weight, "tp", axis=1, tiled=True)
    key_rows = fill_cols(token_rows, key_piece)
    value_rows = fill_cols(token_rows, value_piece)
    own_columns = local_new(new_token, query_proj_matrix, key_weight, value_weight)
    queries, new_keys, new_values = (
        lax.all_gather(own_columns[0], "tp", axis=1, tiled=True),
        lax.all_gather(own_columns[1], "tp", axis=1, tiled=True),
        lax.all_gather(own_columns[2], "tp", axis=1, tiled=True),
    )
    slot_count = seq_count * span_count
    cached_keys, cached_values = (
        lax.all_to_all(
            key_rows.reshape(slot_count, piece_rows, key_width),
            "sp",
            split_axis=0,
            concat_axis=1,
            tiled=True,
        ),
        lax.all_to_all(
            value_rows.reshape(slot_count, piece_rows, value_width),
            "sp",
            split_axis=0,
            concat_axis=1,
            tiled=True,
        ),
    )
    block_rows = cached_keys.shape[1]
    key_cache = cached_keys.reshape(1, 1, block_rows, key_width)
    value_cache = cached_values.reshape(1, 1, block_rows, value_width)
    all_queries = queries.reshape(seq_count, HEADS, 2, MAP_HEAD_SIZE)
    own_seq = lax.axis_index("sp") // span_count
    own_query = lax.dynamic_slice_in_dim(all_queries, own_seq, 1, 0)
    peak, totals, weighted = partial_read(
        own_query,
        cached_keys.reshape(1, block_rows, HEADS, 2, MAP_HEAD_SIZE),
        cached_values.reshape(1, block_rows, HEADS, VD),
    )
    chosen = jnp.arange(seq_count) == own_seq
    chosen_rows = chosen[:, None, None]
    spread = (
        jnp.where(chosen_rows, peak, far_below),
        jnp.where(chosen_rows, totals, 0.0),
        jnp.where(chosen_rows[..., None], weighted, 0.0),
    )
    merged = joined(spread, ("sp", "tp"), combine)
    own_keys = new_keys.reshape(seq_count, HEADS, 2, MAP_HEAD_SIZE)
    own_score = jnp.einsum(
        "bhmd,bhmd->bhm", all_queries, own_keys, preferred_element_type=jnp.float32
    ) * MAP_HEAD_SIZE ** (-0.5)
    own_values = new_values.astype(jnp.float32).reshape(seq_count, HEADS, VD)
    own_weighted = jnp.broadcast_to(own_values[:, :, None, :], (seq_count, HEADS, 2, VD))
    own_state = (own_score, jnp.ones_like(own_score), own_weighted)
    _, totals, weighted = combine(merged, own_state)
    heads_out = weighted / totals[..., None]
    blended = heads_out[:, :, 0] - map_balance[None, :, None] * heads_out[:, :, 1]
    normed = (
        blended
        * lax.rsqrt(jnp.mean(blended * blended, axis=-1, keepdims=True) + norm_eps)
        * head_gain
    )
    return (key_cache, value_cache, normed.reshape(seq_count, HEADS * VD))


MESH = pl.DeviceIdType.MESH
CORES = 2
PIECES = 2


def merged(states):
    peak = functools.reduce(jnp.maximum, [a[1] for a in states])
    factors = [jnp.exp(a[1] - peak) for a in states]
    weighted = functools.reduce(jnp.add, [a[0] * f for a, f in zip(states, factors)])
    total = functools.reduce(jnp.add, [a[2] * f for a, f in zip(states, factors)])
    return weighted, peak, total


def pack(ref, state):
    weighted, peak, total = state
    rows = weighted.shape[0]
    lane = lax.broadcasted_iota(jnp.int32, weighted.shape, 1)
    ref[:rows] = weighted
    ref[rows:] = jnp.where(lane < VD // 2, peak, total)


def unpack(ref):
    rows = ref.shape[0] // 2
    tail = ref[rows:]
    return ref[:rows], tail[:, :1], tail[:, VD // 2 : VD // 2 + 1]


def step_kernel(
    dims,
    prompt, token_hbm, wq_hbm, wk_hbm, wv_hbm, balance_hbm, gain_hbm,
    kv, read,
    xbuf, wbuf, kvbuf, wq, token, balance, gain, qbuf, pbuf, pstat, stbuf, finbuf,
    loc, line_send, prim_recv, xy_send, sec_recv, sib_send, sib_recv,
    out_send, out_recv, pk_send, pk_recv, st_send, st_recv, fin_send, fin_recv,
):
    sp_count, tp_count, seq_count = dims
    _, _, depth, wide = wbuf.shape
    cols = wide // CORES
    chips = tp_count // CORES
    rows = xbuf.shape[1]
    state_rows = CORES * 2 * seq_count
    s = lax.axis_index("sp")
    t = lax.axis_index("tp")
    z = t // CORES
    c = t % CORES
    sib = z * CORES + (1 - c)
    xs = s + 1 - 2 * (s % 2)
    ys = (s + 2) % 4
    diag = 3 - s
    prim = (s + s // 2) % 2
    sec = 1 - prim
    half = depth // 2
    step = half // PIECES
    part_rows = step // 2

    def lanes_of(core):
        return pl.ds(pl.multiple_of(core * cols, cols), cols)

    lanes, sib_lanes = lanes_of(c), lanes_of(1 - c)

    loads = [
        pltpu.make_async_copy(wk_hbm, wbuf.at[0, z, :, lanes], loc.at[0]),
        pltpu.make_async_copy(wv_hbm, wbuf.at[1, z, :, lanes], loc.at[1]),
        pltpu.make_async_copy(prompt, xbuf, loc.at[2]),
        pltpu.make_async_copy(token_hbm, token, loc.at[3]),
        pltpu.make_async_copy(wq_hbm, wq, loc.at[4]),
        pltpu.make_async_copy(balance_hbm, balance, loc.at[5]),
        pltpu.make_async_copy(gain_hbm, gain, loc.at[6]),
    ]
    for a in loads:
        a.start()

    peers = [(s, (t + d) % tp_count) for d in range(1, tp_count)]
    z_peers = [(s, (t + d * CORES) % tp_count) for d in range(1, chips)]
    plane_peers = [((s + d) % sp_count, t) for d in range(1, sp_count)]
    cross_peers = [((s + d) % sp_count, sib) for d in range(1, sp_count)]
    barrier = pltpu.get_barrier_semaphore()
    greeted = peers + plane_peers + cross_peers
    for p in greeted:
        pl.semaphore_signal(barrier, inc=1, device_id=p, device_id_type=MESH)
    pl.semaphore_wait(barrier, len(greeted))

    def remote(src, dst, send, recv, dev):
        return pltpu.make_async_remote_copy(
            src_ref=src, dst_ref=dst, send_sem=send, recv_sem=recv, device_id=dev, device_id_type=MESH
        )

    def push(view, send, recv, dev):
        remote(view, view, send, recv, dev).start()

    def got(view, recv):
        remote(view, view, xy_send, recv, (s, sib)).wait_recv()

    def gone(view, send):
        remote(view, view, send, loc.at[0], (s, sib)).wait_send()

    def span(start, size):
        return pl.ds(pl.multiple_of(start, size), size)

    def piece_of(m, zz, p):
        return wbuf.at[m, zz, span(prim * half + p * step, step), lanes]

    def line(direction, m, zz, p):
        view = piece_of(m, zz, p)
        push(view, line_send.at[(direction + 1) // 2], prim_recv.at[m, zz, p], (s, t + direction * CORES))

    def has_next(direction):
        return (z > 0) if direction < 0 else (z < chips - 1)

    for m in range(2):
        loads[m].wait()
        for direction in (-1, 1):
            @pl.when(has_next(direction))
            def _(direction=direction, m=m):
                for p in range(PIECES):
                    line(direction, m, z, p)
        push(wbuf.at[m, z, :, lanes], sib_send, sib_recv.at[m, z], (s, sib))

    loads[3].wait()
    loads[4].wait()
    vector = token[...]
    me_q = jnp.dot(vector, wq[...], preferred_element_type=jnp.float32)
    me_k = jnp.dot(vector, wbuf[0, z, :, lanes], preferred_element_type=jnp.float32)
    me_v = jnp.dot(vector, wbuf[1, z, :, lanes], preferred_element_type=jnp.float32)
    for i, value in enumerate((me_q, me_k, me_v)):
        value = value.astype(jnp.bfloat16).astype(jnp.float32)
        qbuf[t, i * seq_count : (i + 1) * seq_count, :] = value[:seq_count]

    near = jnp.minimum(z, chips - 1 - z)
    inside = near > 0

    def source(j):
        j = j + 1
        paired = j <= 2 * near
        dist = jnp.where(paired, (j + 1) // 2, j - near)
        from_left = jnp.where(paired, j % 2 == 1, z > near)
        return jnp.where(from_left, z - dist, z + dist), from_left

    def event(e):
        both = jnp.logical_and(inside, e < 8)
        j = jnp.where(both, e % 2, e // 4)
        m = jnp.where(both, e // 4, (e // 2) % 2)
        p = jnp.where(both, (e // 2) % 2, e % 2)
        return j, m, p

    def group(g):
        both = jnp.logical_and(inside, g < 4)
        return jnp.where(both, g % 2, g // 2), jnp.where(both, g // 2, g % 2)

    def arrive(e):
        j, m, p = event(e)
        zz, from_left = source(j)
        view = piece_of(m, zz, p)
        got(view, prim_recv.at[m, zz, p])
        on_right = jnp.logical_and(from_left, z < chips - 1)
        on_left = jnp.logical_and(jnp.logical_not(from_left), z > 0)
        pl.when(on_right)(lambda: line(1, m, zz, p))
        pl.when(on_left)(lambda: line(-1, m, zz, p))
        for h, to in enumerate((xs, ys)):
            part = wbuf.at[m, zz, span(prim * half + p * step + h * part_rows, part_rows), lanes]
            push(part, xy_send, sec_recv.at[m, zz], (to, t))
        push(view, sib_send, sib_recv.at[m, zz], (s, sib))

    def arrive_secondary(g):
        j, m = group(g)
        zz, _ = source(j)
        view = wbuf.at[m, zz, span(sec * half, half), lanes]
        got(view, sec_recv.at[m, zz])
        push(view, sib_send, sib_recv.at[m, zz], (s, sib))

    def columns_of(zz):
        return pl.ds(pl.multiple_of(zz * wide, wide), wide)

    def multiply(m, zz):
        got(wbuf.at[m, zz, :, sib_lanes], sib_recv.at[m, zz])
        columns = columns_of(zz)

        def some(i, _):
            at = pl.ds(2 * i, 2)
            product = jnp.dot(
                xbuf[at].reshape(-1, depth), wbuf[m, zz], preferred_element_type=jnp.float32
            ).astype(jnp.bfloat16)
            kvbuf[m, at, :, columns] = product.reshape(2, rows, wide)
            return 0

        lax.fori_loop(0, sp_count // 2, some, 0)
        kv[m, span(s * rows, rows), columns] = kvbuf[m, s, :, columns]

    def send_results(m, zz):
        columns = columns_of(zz)
        for p in (diag, xs, ys):
            remote(
                kvbuf.at[m, p, :, columns], kv.at[m, span(s * rows, rows), columns],
                out_send, out_recv, (p, t),
            ).start()

    scale = MAP_HEAD_SIZE ** (-0.5)
    row = lax.broadcasted_iota(jnp.int32, (state_rows, 1), 0)
    row_map = row // (CORES * seq_count)
    row_seq = (row // CORES) % seq_count
    row_head = row % CORES

    def by_seq(new, first):
        values = jnp.zeros((state_rows, new.shape[1]), jnp.float32)
        for b in range(seq_count):
            values = jnp.where(row_seq == b, new[first + b : first + b + 1], values)
        return values

    def by_head(values):
        return functools.reduce(
            jnp.add,
            [jnp.where(row_head == i, values[:, i * VD : (i + 1) * VD], 0.0) for i in range(CORES)],
        )

    def new_rows(zz):
        return jnp.concatenate([qbuf[zz * CORES + i] for i in range(CORES)], axis=1)

    def query_of(new):
        lane = lax.broadcasted_iota(jnp.int32, (state_rows, wide), 1)
        mine = lane // MAP_HEAD_SIZE == row_head * 2 + row_map
        return jnp.where(mine, by_seq(new, 0), 0.0)

    def score(j, zz):
        query = query_of(new_rows(zz)).astype(jnp.bfloat16)
        keys = kvbuf[0, :, :, columns_of(zz)].reshape(-1, wide)
        scores = lax.dot_general(
            query, keys, (((1,), (1,)), ((), ())), preferred_element_type=jnp.float32
        ) * scale
        at = lax.broadcasted_iota(jnp.int32, scores.shape, 1)
        mine = at // (scores.shape[1] // seq_count) == row_seq
        peak = jnp.max(jnp.where(mine, scores, far_below), axis=1, keepdims=True)
        raised = jnp.where(mine, jnp.exp(scores - peak), 0.0)
        total = jnp.sum(raised, axis=1, keepdims=True)
        high = raised.astype(jnp.bfloat16)
        low = (raised - high.astype(jnp.float32)).astype(jnp.bfloat16)
        pbuf[j, :state_rows] = high
        pbuf[j, state_rows:] = low
        pstat[j, 0] = jnp.broadcast_to(peak, (state_rows, VD))
        pstat[j, 1] = jnp.broadcast_to(total, (state_rows, VD))

    def weigh(j, zz):
        values = kvbuf[1, :, :, columns_of(zz)].reshape(-1, wide)
        both = jnp.dot(pbuf[j], values, preferred_element_type=jnp.float32)
        return by_head(both[:state_rows] + both[state_rows:]), pstat[j, 0][:, :1], pstat[j, 1][:, :1]

    def send_state(zz):
        view = stbuf.at[z, zz]
        for p in z_peers:
            push(view, st_send, st_recv.at[zz], p)

    mine_at = chips - 1
    loads[2].wait()
    multiply(0, z)
    for p in peers:
        push(qbuf.at[t], pk_send, pk_recv.at[t], p)
    send_results(0, z)
    multiply(1, z)
    got(qbuf.at[sib], pk_recv.at[sib])
    score(mine_at, z)
    send_results(1, z)
    new = new_rows(z)
    own_score = jnp.sum(query_of(new) * by_seq(new, seq_count), axis=1, keepdims=True) * scale
    holder = jnp.logical_and(s == 0, c == 0)
    own = (
        jnp.where(holder, by_head(by_seq(new, 2 * seq_count)), 0.0),
        jnp.where(holder, own_score, far_below),
        jnp.where(holder, jnp.ones_like(own_score), 0.0),
    )
    pack(stbuf.at[z, z], merged([weigh(mine_at, z), own]))

    def finish(g):
        j, m = group(g)
        zz, _ = source(j)
        multiply(m, zz)

        @pl.when(m == 0)
        def _():
            for i in range(CORES):
                got(qbuf.at[zz * CORES + i], pk_recv.at[zz * CORES + i])
            score(j, zz)
            send_results(m, zz)

        @pl.when(m == 1)
        def _():
            pack(stbuf.at[z, zz], weigh(j, zz))
            send_results(m, zz)
            send_state(zz)

    arrive(0)
    send_state(z)
    arrive(1)
    groups = 2 * (chips - 1)

    def work(g, _):
        arrive(2 * g)
        arrive_secondary(g - 1)
        arrive(2 * g + 1)
        finish(g - 1)
        return 0

    lax.fori_loop(1, groups, work, 0)

    me = s * CORES + c
    ends = (0, chips - 1)
    middle = tuple(range(1, chips - 1))

    def join_z(k, blocks):
        for i, zz in enumerate(blocks):
            got(stbuf.at[pl.ds(0, chips - 1), zz], st_recv.at[zz])
            pack(finbuf.at[k, me, i], merged([unpack(stbuf.at[a, zz]) for a in range(chips)]))
        for p in plane_peers + cross_peers + [(s, sib)]:
            push(finbuf.at[k, me], fin_send, fin_recv.at[k], p)

    join_z(0, middle)
    arrive_secondary(groups - 1)
    finish(groups - 1)
    join_z(1, ends)

    loads[5].wait()
    loads[6].wait()
    others = sp_count * CORES - 1
    fold = state_rows // 2
    for k, blocks in ((0, middle), (1, ends)):
        got(finbuf.at[k, pl.ds(0, others)], fin_recv.at[k])
        for i, zz in enumerate(blocks):
            weighted, _, total = merged([unpack(finbuf.at[k, a, i]) for a in range(others + 1)])
            heads_out = weighted / total
            lane = lax.broadcasted_iota(jnp.int32, (fold, HEADS), 1)
            chosen = lane == zz * CORES + lax.broadcasted_iota(jnp.int32, (fold, HEADS), 0) % CORES
            second = jnp.sum(jnp.where(chosen, balance[...], 0.0), axis=1, keepdims=True)
            blended = heads_out[:fold] - second * heads_out[fold:]
            normed = (
                blended
                * lax.rsqrt(jnp.mean(blended * blended, axis=1, keepdims=True) + norm_eps)
                * gain[...]
            )
            for b in range(seq_count):
                for h in range(CORES):
                    r = b * CORES + h
                    read[b : b + 1, (zz * CORES + h) * VD : (zz * CORES + h + 1) * VD] = normed[r : r + 1]

    others_rows = pl.ds(0, sp_count - 1)
    got(kvbuf.at[:, others_rows], out_recv)
    gone(kvbuf.at[:, others_rows], out_send)
    gone(wbuf.at[0, pl.ds(0, chips - 1), :, lanes], xy_send)
    gone(wbuf.at[:, :, :, lanes], sib_send)
    gone(qbuf.at[pl.ds(0, tp_count - 1)], pk_send)
    gone(stbuf.at[pl.ds(0, chips - 1)], st_send)
    gone(finbuf.at[:, pl.ds(0, others)], fin_send)
    for direction, count in ((-1, chips - z), (1, z + 1)):
        for n in range(1, chips):
            @pl.when(jnp.logical_and(has_next(direction), count == n))
            def _(direction=direction, n=n):
                gone(
                    wbuf.at[:, pl.ds(0, n), pl.ds(0, half), lanes],
                    line_send.at[(direction + 1) // 2],
                )


def store_kernel(kv, read, keys_out, values_out, read_out, sem):
    copies = [
        pltpu.make_async_copy(kv.at[0], keys_out, sem.at[0]),
        pltpu.make_async_copy(kv.at[1], values_out, sem.at[1]),
        pltpu.make_async_copy(read, read_out, sem.at[2]),
    ]
    for a in copies:
        a.start()
    for a in copies:
        a.wait()


def fused(prompt, new_token, query_proj_matrix, key_weight, value_weight, map_balance, head_gain):
    seq_count, _, span_count, _, piece_rows, width = prompt.shape
    sp_count, tp_count = lax.axis_size("sp"), lax.axis_size("tp")
    cols = key_weight.shape[1]
    slots = seq_count * span_count
    chips = tp_count // CORES
    key_width = cols * tp_count
    block_rows = sp_count * piece_rows
    state_rows = CORES * 2 * seq_count
    any_space = pl.BlockSpec(memory_space=pltpu.HBM)
    vmem = pl.BlockSpec(memory_space=pltpu.VMEM)
    dma = pltpu.SemaphoreType.DMA
    kv, read = pl.pallas_call(
        functools.partial(step_kernel, (sp_count, tp_count, seq_count)),
        out_shape=[
            pltpu.VMEM((2, block_rows, key_width), jnp.bfloat16),
            pltpu.VMEM((seq_count, HEADS * VD), jnp.float32),
        ],
        in_specs=[any_space] * 7,
        out_specs=[vmem, vmem],
        scratch_shapes=[
            pltpu.VMEM((slots, piece_rows, width), jnp.bfloat16),
            pltpu.VMEM((2, chips, width, CORES * cols), jnp.bfloat16),
            pltpu.VMEM((2, slots, piece_rows, key_width), jnp.bfloat16),
            pltpu.VMEM((width, cols), jnp.bfloat16),
            pltpu.VMEM((seq_count, width), jnp.bfloat16),
            pltpu.VMEM((1, HEADS), jnp.float32),
            pltpu.VMEM((1, VD), jnp.float32),
            pltpu.VMEM((tp_count, 8, cols), jnp.float32),
            pltpu.VMEM((chips, 2 * state_rows, slots * piece_rows), jnp.bfloat16),
            pltpu.VMEM((chips, 2, state_rows, VD), jnp.float32),
            pltpu.VMEM((chips, chips, 2 * state_rows, VD), jnp.float32),
            pltpu.VMEM((2, sp_count * CORES, 2, 2 * state_rows, VD), jnp.float32),
            dma((7,)), dma((2,)), dma((2, chips, PIECES)), dma(()), dma((2, chips)),
            dma(()), dma((2, chips)),
            dma(()), dma(()), dma(()), dma((tp_count,)), dma(()), dma((chips,)), dma(()), dma((2,)),
        ],
        compiler_params=pltpu.CompilerParams(
            collective_id=0, has_side_effects=True, vmem_limit_bytes=61 * 1024 * 1024 + 800 * 1024
        ),
    )(
        prompt.reshape(slots, piece_rows, width),
        new_token, query_proj_matrix, key_weight, value_weight,
        map_balance[None, :], head_gain[None, :],
    )
    keys, values, read = pl.pallas_call(
        store_kernel,
        out_shape=[
            jax.ShapeDtypeStruct((block_rows, key_width), jnp.bfloat16),
            jax.ShapeDtypeStruct((block_rows, key_width), jnp.bfloat16),
            jax.ShapeDtypeStruct(read.shape, jnp.float32),
        ],
        in_specs=[vmem, vmem],
        out_specs=[any_space] * 3,
        scratch_shapes=[dma((3,))],
        compiler_params=pltpu.CompilerParams(vmem_limit_bytes=1024 * 1024),
    )(kv, read)
    shape = (1, 1, block_rows, key_width)
    return keys.reshape(shape), values.reshape(shape), read


def fits(mesh, key_weight, value_weight, prompt):
    tp_count, sp_count = mesh.shape["tp"], mesh.shape["sp"]
    seq_count, _, span_count = prompt.shape[:3]
    cols = key_weight.shape[1] // tp_count
    return (
        sp_count == 4
        and seq_count * span_count == sp_count
        and tp_count % CORES == 0
        and tp_count == 4 * CORES
        and cols == VD
        and 3 * seq_count <= 8
        and key_weight.shape == value_weight.shape
    )


def solution(mesh):
    in_specs = (
        P(None, "tp", None, "sp", None, None),
        P(),
        P(None, "tp"),
        P(None, "tp"),
        P(None, "tp"),
        P(),
        P(),
    )
    out_specs = (P("sp", "tp", None, None), P("sp", "tp", None, None), P())

    def step(prompt, new_token, query_proj_matrix, key_weight, value_weight, map_balance, head_gain):
        body = fused if fits(mesh, key_weight, value_weight, prompt) else shards
        mapped = jax.shard_map(
            body, mesh=mesh, in_specs=in_specs, out_specs=out_specs, check_vma=False
        )
        return mapped(
            prompt, new_token, query_proj_matrix, key_weight, value_weight, map_balance, head_gain
        )

    return step
```

time: 62.9 us -> 66.7 us (1.060)
  Pallas kernels: 59.6 us -> 65.9 us
  local copies, waits for them, and re-layouts: 2.54 us -> 0 us
    pallas_call x1, Pallas kernels: 59.6 us -> 64.5 us  [fused(): pl.pallas_call(functools.partial(step_kernel, (sp_count, tp_count, seq_co...]
    unnamed x3 -> x0, local copies, waits for them, and re-layouts: 2.54 us -> none
    pallas_call x0 -> x1, Pallas kernels: none -> 1.35 us  [fused(): pl.pallas_call(store_kernel, out_shape=[jax.ShapeDtypeStruct((block_rows,...]
where the time goes in v1:
time: 66.7 us; the launch traced here: 66.5 us
  Pallas kernels  65.9 us (99%)
    pallas_call x1, Pallas kernels, fused(): pl.pallas_call(functools.partial(step_kernel, (sp_count, tp_count, seq_co...  64.5 us
    pallas_call x1, Pallas kernels, fused(): pl.pallas_call(store_kernel, out_shape=[jax.ShapeDtypeStruct((block_rows,...  1.35 us

profile of v1, /device:TPU:0, one launch (start us, length us, event | category | flops | bytes accessed | tf_op | source)
XLA Modules:
  0.0 66.5 jit_solution(11964017277518493518)
XLA Ops:
  0.6 64.5 %shard_map.94 = (bf16[2,512,1024]{2,1,0:T(8,128)(2,1)S(1)}, f32[2,1024]{1,0:T(2,128)S(1)}) custom-call(bf16[4,128,2048]{2,1,0:T(8,128)(2,1)} %bitcast.5, bf16[2,2048]{1,0:T(2,128)(2,1)} %token_hbm.1, bf16[2048,128]{1,0:T(8,128)(2,1)} %wq_hbm.1, bf16[2048,128]{1,0:T(8,128)(2,1)} %wk_hbm.1, bf16[2048,128]{1,0:T(8,128)(2,1)} %wv_hbm.1, f32[1,8]{1,0:T(1,128)} %bitcast.6, ...), custom_call_target="tpu_custom_call" | custom-call | tf_op jit(solution)/shard_map/pallas_call | solution.py:522
  65.2 1.3 %shard_map.95 = (bf16[512,1024]{1,0:T(8,128)(2,1)}, bf16[512,1024]{1,0:T(8,128)(2,1)}, f32[2,1024]{1,0:T(2,128)}) custom-call(bf16[2,512,1024]{2,1,0:T(8,128)(2,1)S(1)} %get-tuple-element.8.kv, f32[2,1024]{1,0:T(2,128)S(1)} %get-tuple-element.9.read), custom_call_target="tpu_custom_call" | custom-call | tf_op jit(solution)/shard_map/pallas_call | solution.py:555

commit v2 on v1

--- a/solution.py
+++ b/solution.py
@@ -149,26 +149,32 @@
     return weighted, peak, total
 
 
-def pack(ref, state):
+def pack(ref, at, stat_at, state):
     weighted, peak, total = state
     rows = weighted.shape[0]
     lane = lax.broadcasted_iota(jnp.int32, weighted.shape, 1)
-    ref[:rows] = weighted
-    ref[rows:] = jnp.where(lane < VD // 2, peak, total)
-
-
-def unpack(ref):
-    rows = ref.shape[0] // 2
-    tail = ref[rows:]
-    return ref[:rows], tail[:, :1], tail[:, VD // 2 : VD // 2 + 1]
+    row = lax.broadcasted_iota(jnp.int32, weighted.shape, 0)
+    stats = jnp.where(lane == row, peak, jnp.where(lane == row + rows, total, 0.0))
+    ref[at : at + rows] = weighted
+    ref[stat_at : stat_at + 1] = jnp.sum(stats, axis=0, keepdims=True)
+
+
+def unpack(ref, at, stat_at, rows):
+    weighted = ref[at : at + rows]
+    lane = lax.broadcasted_iota(jnp.int32, weighted.shape, 1)
+    row = lax.broadcasted_iota(jnp.int32, weighted.shape, 0)
+    stats = ref[stat_at : stat_at + 1]
+    peak = jnp.sum(jnp.where(lane == row, stats, 0.0), axis=1, keepdims=True)
+    total = jnp.sum(jnp.where(lane == row + rows, stats, 0.0), axis=1, keepdims=True)
+    return weighted, peak, total
 
 
 def step_kernel(
     dims,
-    prompt, token_hbm, wq_hbm, wk_hbm, wv_hbm, balance_hbm, gain_hbm,
-    kv, read,
-    xbuf, wbuf, kvbuf, wq, token, balance, gain, qbuf, pbuf, pstat, stbuf, finbuf,
-    loc, line_send, prim_recv, xy_send, sec_recv, sib_send, sib_recv,
+    prompt, token_hbm, wq_hbm, wk_hbm, wv_hbm,
+    kv, finbuf,
+    xbuf, wbuf, kvbuf, wq, token, qbuf, pbuf, pstat, stbuf,
+    loc, far_send, far_recv, line_send, prim_recv, xy_send, sec_recv, sib_send, sib_recv,
     out_send, out_recv, pk_send, pk_recv, st_send, st_recv, fin_send, fin_recv,
 ):
     sp_count, tp_count, seq_count = dims
@@ -199,11 +205,11 @@
     loads = [
         pltpu.make_async_copy(wk_hbm, wbuf.at[0, z, :, lanes], loc.at[0]),
         pltpu.make_async_copy(wv_hbm, wbuf.at[1, z, :, lanes], loc.at[1]),
-        pltpu.make_async_copy(prompt, xbuf, loc.at[2]),
-        pltpu.make_async_copy(token_hbm, token, loc.at[3]),
-        pltpu.make_async_copy(wq_hbm, wq, loc.at[4]),
-        pltpu.make_async_copy(balance_hbm, balance, loc.at[5]),
-        pltpu.make_async_copy(gain_hbm, gain, loc.at[6]),
+        pltpu.make_async_copy(prompt.at[xs], xbuf.at[0], loc.at[2]),
+        pltpu.make_async_copy(prompt.at[ys], xbuf.at[1], loc.at[3]),
+        pltpu.make_async_copy(token_hbm, token, loc.at[4]),
+        pltpu.make_async_copy(wq_hbm, wq, loc.at[5]),
+        pltpu.make_async_copy(prompt.at[s], xbuf.at[2], loc.at[6]),
     ]
     for a in loads:
         a.start()
@@ -245,6 +251,8 @@
     def has_next(direction):
         return (z > 0) if direction < 0 else (z < chips - 1)
 
+    far_prompt = remote(prompt.at[diag], xbuf.at[3], far_send, far_recv, (diag, t))
+    far_prompt.start()
     for m in range(2):
         loads[m].wait()
         for direction in (-1, 1):
@@ -253,16 +261,6 @@
                 for p in range(PIECES):
                     line(direction, m, z, p)
         push(wbuf.at[m, z, :, lanes], sib_send, sib_recv.at[m, z], (s, sib))
-
-    loads[3].wait()
-    loads[4].wait()
-    vector = token[...]
-    me_q = jnp.dot(vector, wq[...], preferred_element_type=jnp.float32)
-    me_k = jnp.dot(vector, wbuf[0, z, :, lanes], preferred_element_type=jnp.float32)
-    me_v = jnp.dot(vector, wbuf[1, z, :, lanes], preferred_element_type=jnp.float32)
-    for i, value in enumerate((me_q, me_k, me_v)):
-        value = value.astype(jnp.bfloat16).astype(jnp.float32)
-        qbuf[t, i * seq_count : (i + 1) * seq_count, :] = value[:seq_count]
 
     near = jnp.minimum(z, chips - 1 - z)
     inside = near > 0
@@ -309,26 +307,34 @@
     def columns_of(zz):
         return pl.ds(pl.multiple_of(zz * wide, wide), wide)
 
+    def product(pair, m, zz, first, width):
+        at = pl.ds(2 * pair, 2)
+        columns = span(zz * wide + first, width)
+        out = jnp.dot(
+            xbuf[at].reshape(-1, depth), wbuf[m, zz, :, span(first, width)],
+            preferred_element_type=jnp.float32,
+        ).astype(jnp.bfloat16)
+        kvbuf[m, at, :, columns] = out.reshape(2, rows, width)
+        return columns
+
+    def keep(m, columns):
+        for i, slot in ((2, s), (3, diag)):
+            kv[m, span(slot * rows, rows), columns] = kvbuf[m, i, :, columns]
+
     def multiply(m, zz):
         got(wbuf.at[m, zz, :, sib_lanes], sib_recv.at[m, zz])
-        columns = columns_of(zz)
-
-        def some(i, _):
-            at = pl.ds(2 * i, 2)
-            product = jnp.dot(
-                xbuf[at].reshape(-1, depth), wbuf[m, zz], preferred_element_type=jnp.float32
-            ).astype(jnp.bfloat16)
-            kvbuf[m, at, :, columns] = product.reshape(2, rows, wide)
+
+        def some(pair, _):
+            product(pair, m, zz, 0, wide)
             return 0
 
-        lax.fori_loop(0, sp_count // 2, some, 0)
-        kv[m, span(s * rows, rows), columns] = kvbuf[m, s, :, columns]
-
-    def send_results(m, zz):
-        columns = columns_of(zz)
-        for p in (diag, xs, ys):
+        lax.fori_loop(0, 2, some, 0)
+        keep(m, columns_of(zz))
+
+    def send_columns(m, columns):
+        for i, p in enumerate((xs, ys)):
             remote(
-                kvbuf.at[m, p, :, columns], kv.at[m, span(s * rows, rows), columns],
+                kvbuf.at[m, i, :, columns], kv.at[m, span(s * rows, rows), columns],
                 out_send, out_recv, (p, t),
             ).start()
 
@@ -364,8 +370,10 @@
         scores = lax.dot_general(
             query, keys, (((1,), (1,)), ((), ())), preferred_element_type=jnp.float32
         ) * scale
-        at = lax.broadcasted_iota(jnp.int32, scores.shape, 1)
-        mine = at // (scores.shape[1] // seq_count) == row_seq
+        at = lax.broadcasted_iota(jnp.int32, scores.shape, 1) // rows
+        spans = sp_count // seq_count
+        owner = jnp.where(at == 0, xs, jnp.where(at == 1, ys, s)) // spans
+        mine = owner == row_seq
         peak = jnp.max(jnp.where(mine, scores, far_below), axis=1, keepdims=True)
         raised = jnp.where(mine, jnp.exp(scores - peak), 0.0)
         total = jnp.sum(raised, axis=1, keepdims=True)
@@ -382,31 +390,56 @@
         return by_head(both[:state_rows] + both[state_rows:]), pstat[j, 0][:, :1], pstat[j, 1][:, :1]
 
     def send_state(zz):
-        view = stbuf.at[z, zz]
+        view = stbuf.at[z, zz, pl.ds(0, state_rows + 1)]
         for p in z_peers:
             push(view, st_send, st_recv.at[zz], p)
 
     mine_at = chips - 1
     loads[2].wait()
-    multiply(0, z)
-    for p in peers:
-        push(qbuf.at[t], pk_send, pk_recv.at[t], p)
-    send_results(0, z)
-    multiply(1, z)
-    got(qbuf.at[sib], pk_recv.at[sib])
-    score(mine_at, z)
-    send_results(1, z)
-    new = new_rows(z)
-    own_score = jnp.sum(query_of(new) * by_seq(new, seq_count), axis=1, keepdims=True) * scale
-    holder = jnp.logical_and(s == 0, c == 0)
-    own = (
-        jnp.where(holder, by_head(by_seq(new, 2 * seq_count)), 0.0),
-        jnp.where(holder, own_score, far_below),
-        jnp.where(holder, jnp.ones_like(own_score), 0.0),
-    )
-    pack(stbuf.at[z, z], merged([weigh(mine_at, z), own]))
-
-    def finish(g):
+    loads[3].wait()
+    before = None
+    for core in (c, 1 - c):
+        for m in range(2):
+            if core is not c:
+                got(wbuf.at[m, z, :, sib_lanes], sib_recv.at[m, z])
+            columns = product(0, m, z, core * cols, cols)
+            if before is not None:
+                send_columns(*before)
+            before = (m, columns)
+
+    def vectors():
+        loads[4].wait()
+        loads[5].wait()
+        vector = token[...]
+        me_q = jnp.dot(vector, wq[...], preferred_element_type=jnp.float32)
+        me_k = jnp.dot(vector, wbuf[0, z, :, lanes], preferred_element_type=jnp.float32)
+        me_v = jnp.dot(vector, wbuf[1, z, :, lanes], preferred_element_type=jnp.float32)
+        for i, value in enumerate((me_q, me_k, me_v)):
+            value = value.astype(jnp.bfloat16).astype(jnp.float32)
+            qbuf[t, i * seq_count : (i + 1) * seq_count, :] = value[:seq_count]
+    def own_block():
+        loads[6].wait()
+        far_prompt.wait_recv()
+
+        def some(m, _):
+            product(1, m, z, 0, wide)
+            keep(m, columns_of(z))
+            return 0
+
+        lax.fori_loop(0, 2, some, 0)
+        got(qbuf.at[sib], pk_recv.at[sib])
+        score(mine_at, z)
+        new = new_rows(z)
+        own_score = jnp.sum(query_of(new) * by_seq(new, seq_count), axis=1, keepdims=True) * scale
+        holder = jnp.logical_and(s == 0, c == 0)
+        own = (
+            jnp.where(holder, by_head(by_seq(new, 2 * seq_count)), 0.0),
+            jnp.where(holder, own_score, far_below),
+            jnp.where(holder, jnp.ones_like(own_score), 0.0),
+        )
+        pack(stbuf.at[z, z], 0, state_rows, merged([weigh(mine_at, z), own]))
+
+    def compute(g):
         j, m = group(g)
         zz, _ = source(j)
         multiply(m, zz)
@@ -416,27 +449,61 @@
             for i in range(CORES):
                 got(qbuf.at[zz * CORES + i], pk_recv.at[zz * CORES + i])
             score(j, zz)
-            send_results(m, zz)
 
         @pl.when(m == 1)
         def _():
-            pack(stbuf.at[z, zz], weigh(j, zz))
-            send_results(m, zz)
-            send_state(zz)
-
-    arrive(0)
-    send_state(z)
-    arrive(1)
+            pack(stbuf.at[z, zz], 0, state_rows, weigh(j, zz))
+
+    def results(g):
+        j, m = group(g)
+        zz, _ = source(j)
+        send_columns(m, columns_of(zz))
+
+    def state(g):
+        j, m = group(g)
+        zz, _ = source(j)
+        pl.when(m == 1)(lambda: send_state(zz))
+
     groups = 2 * (chips - 1)
-
-    def work(g, _):
-        arrive(2 * g)
-        arrive_secondary(g - 1)
-        arrive(2 * g + 1)
-        finish(g - 1)
+    def finish(g):
+        compute(g)
+        results(g)
+        state(g)
+
+    own_at = jnp.where(inside, 7, 4)
+
+    def work(e, _):
+        arrive(e)
+
+        @pl.when(e == 0)
+        def _():
+            send_columns(*before)
+            vectors()
+
+        @pl.when(e == 1)
+        def _():
+            for p in peers:
+                push(qbuf.at[t], pk_send, pk_recv.at[t], p)
+
+        pl.when(e == own_at)(own_block)
+        pl.when(e == own_at + 1)(lambda: send_state(z))
+        outside = jnp.logical_not(inside)
+        done = jnp.where(e < 9, e - 6, e - 7)
+        pl.when(outside & (e >= 6) & (e != 9))(lambda: finish(done))
+        ready = jnp.where(inside, e - 10, jnp.where(e < 8, e - 5, e - 6))
+        pl.when((ready >= 0) & (inside | ((e != 8) & (e < 11))))(lambda: arrive_secondary(ready))
         return 0
 
-    lax.fori_loop(1, groups, work, 0)
+    events = 2 * groups
+    lax.fori_loop(0, events, work, 0)
+
+    def rest(g, _):
+        finish(g)
+        pl.when(g + 2 < groups)(lambda: arrive_secondary(g + 2))
+        return 0
+
+    lax.fori_loop(0, jnp.where(inside, groups - 1, 0), rest, 0)
+    pl.when(jnp.logical_not(inside))(lambda: arrive_secondary(groups - 1))
 
     me = s * CORES + c
     ends = (0, chips - 1)
@@ -444,47 +511,36 @@
 
     def join_z(k, blocks):
         for i, zz in enumerate(blocks):
-            got(stbuf.at[pl.ds(0, chips - 1), zz], st_recv.at[zz])
-            pack(finbuf.at[k, me, i], merged([unpack(stbuf.at[a, zz]) for a in range(chips)]))
+            got(stbuf.at[pl.ds(0, chips - 1), zz, pl.ds(0, state_rows + 1)], st_recv.at[zz])
+            whole = merged([unpack(stbuf.at[a, zz], 0, state_rows, state_rows) for a in range(chips)])
+            pack(finbuf.at[k, me], i * state_rows, len(blocks) * state_rows + i, whole)
+
+    def send_joined(k, blocks):
+        view = finbuf.at[k, me, pl.ds(0, len(blocks) * (state_rows + 1))]
         for p in plane_peers + cross_peers + [(s, sib)]:
-            push(finbuf.at[k, me], fin_send, fin_recv.at[k], p)
+            push(view, fin_send, fin_recv.at[k], p)
 
     join_z(0, middle)
-    arrive_secondary(groups - 1)
-    finish(groups - 1)
+    compute(groups - 1)
+    send_joined(0, middle)
+    state(groups - 1)
+    results(groups - 1)
     join_z(1, ends)
-
-    loads[5].wait()
-    loads[6].wait()
+    send_joined(1, ends)
     others = sp_count * CORES - 1
-    fold = state_rows // 2
-    for k, blocks in ((0, middle), (1, ends)):
-        got(finbuf.at[k, pl.ds(0, others)], fin_recv.at[k])
-        for i, zz in enumerate(blocks):
-            weighted, _, total = merged([unpack(finbuf.at[k, a, i]) for a in range(others + 1)])
-            heads_out = weighted / total
-            lane = lax.broadcasted_iota(jnp.int32, (fold, HEADS), 1)
-            chosen = lane == zz * CORES + lax.broadcasted_iota(jnp.int32, (fold, HEADS), 0) % CORES
-            second = jnp.sum(jnp.where(chosen, balance[...], 0.0), axis=1, keepdims=True)
-            blended = heads_out[:fold] - second * heads_out[fold:]
-            normed = (
-                blended
-                * lax.rsqrt(jnp.mean(blended * blended, axis=1, keepdims=True) + norm_eps)
-                * gain[...]
-            )
-            for b in range(seq_count):
-                for h in range(CORES):
-                    r = b * CORES + h
-                    read[b : b + 1, (zz * CORES + h) * VD : (zz * CORES + h + 1) * VD] = normed[r : r + 1]
-
-    others_rows = pl.ds(0, sp_count - 1)
+    fin_rows = pl.ds(0, 2 * (state_rows + 1))
+    for k in range(2):
+        got(finbuf.at[k, pl.ds(0, others), fin_rows], fin_recv.at[k])
+
+    others_rows = pl.ds(0, 2)
+    far_prompt.wait_send()
     got(kvbuf.at[:, others_rows], out_recv)
     gone(kvbuf.at[:, others_rows], out_send)
     gone(wbuf.at[0, pl.ds(0, chips - 1), :, lanes], xy_send)
     gone(wbuf.at[:, :, :, lanes], sib_send)
     gone(qbuf.at[pl.ds(0, tp_count - 1)], pk_send)
-    gone(stbuf.at[pl.ds(0, chips - 1)], st_send)
-    gone(finbuf.at[:, pl.ds(0, others)], fin_send)
+    gone(stbuf.at[pl.ds(0, chips - 1), :, pl.ds(0, state_rows + 1)], st_send)
+    gone(finbuf.at[:, pl.ds(0, others), fin_rows], fin_send)
     for direction, count in ((-1, chips - z), (1, z + 1)):
         for n in range(1, chips):
             @pl.when(jnp.logical_and(has_next(direction), count == n))
@@ -495,15 +551,47 @@
                 )
 
 
-def store_kernel(kv, read, keys_out, values_out, read_out, sem):
+def store_kernel(
+    blocks, kv, finbuf, balance_hbm, gain_hbm, keys_out, values_out, read_out, read, balance, gain, sem
+):
     copies = [
-        pltpu.make_async_copy(kv.at[0], keys_out, sem.at[0]),
-        pltpu.make_async_copy(kv.at[1], values_out, sem.at[1]),
-        pltpu.make_async_copy(read, read_out, sem.at[2]),
+        pltpu.make_async_copy(balance_hbm, balance, sem.at[0]),
+        pltpu.make_async_copy(gain_hbm, gain, sem.at[1]),
+        pltpu.make_async_copy(kv.at[0], keys_out, sem.at[2]),
+        pltpu.make_async_copy(kv.at[1], values_out, sem.at[3]),
+        pltpu.make_async_copy(read, read_out, sem.at[4]),
     ]
-    for a in copies:
+    for a in copies[:4]:
         a.start()
-    for a in copies:
+    devices, state_rows = finbuf.shape[1], CORES * 2 * read.shape[0]
+    fold = state_rows // 2
+    seq_count = read.shape[0]
+    heads = {}
+    for k, zz_list in enumerate(blocks):
+        for i, zz in enumerate(zz_list):
+            at, stat_at = i * state_rows, len(zz_list) * state_rows + i
+            weighted, _, total = merged(
+                [unpack(finbuf.at[k, a], at, stat_at, state_rows) for a in range(devices)]
+            )
+            heads[zz] = weighted / total
+    copies[0].wait()
+    copies[1].wait()
+    for zz, heads_out in heads.items():
+        lane = lax.broadcasted_iota(jnp.int32, (fold, HEADS), 1)
+        chosen = lane == zz * CORES + lax.broadcasted_iota(jnp.int32, (fold, HEADS), 0) % CORES
+        second = jnp.sum(jnp.where(chosen, balance[...], 0.0), axis=1, keepdims=True)
+        blended = heads_out[:fold] - second * heads_out[fold:]
+        normed = (
+            blended
+            * lax.rsqrt(jnp.mean(blended * blended, axis=1, keepdims=True) + norm_eps)
+            * gain[...]
+        )
+        for b in range(seq_count):
+            for h in range(CORES):
+                r = b * CORES + h
+                read[b : b + 1, (zz * CORES + h) * VD : (zz * CORES + h + 1) * VD] = normed[r : r + 1]
+    copies[4].start()
+    for a in copies[2:]:
         a.wait()
 
 
@@ -519,13 +607,13 @@
     any_space = pl.BlockSpec(memory_space=pltpu.HBM)
     vmem = pl.BlockSpec(memory_space=pltpu.VMEM)
     dma = pltpu.SemaphoreType.DMA
-    kv, read = pl.pallas_call(
+    kv, states = pl.pallas_call(
         functools.partial(step_kernel, (sp_count, tp_count, seq_count)),
         out_shape=[
             pltpu.VMEM((2, block_rows, key_width), jnp.bfloat16),
-            pltpu.VMEM((seq_count, HEADS * VD), jnp.float32),
+            pltpu.VMEM((2, sp_count * CORES, 2 * state_rows + 8, VD), jnp.float32),
         ],
-        in_specs=[any_space] * 7,
+        in_specs=[any_space] * 5,
         out_specs=[vmem, vmem],
         scratch_shapes=[
             pltpu.VMEM((slots, piece_rows, width), jnp.bfloat16),
@@ -533,37 +621,39 @@
             pltpu.VMEM((2, slots, piece_rows, key_width), jnp.bfloat16),
             pltpu.VMEM((width, cols), jnp.bfloat16),
             pltpu.VMEM((seq_count, width), jnp.bfloat16),
-            pltpu.VMEM((1, HEADS), jnp.float32),
-            pltpu.VMEM((1, VD), jnp.float32),
             pltpu.VMEM((tp_count, 8, cols), jnp.float32),
             pltpu.VMEM((chips, 2 * state_rows, slots * piece_rows), jnp.bfloat16),
             pltpu.VMEM((chips, 2, state_rows, VD), jnp.float32),
             pltpu.VMEM((chips, chips, 2 * state_rows, VD), jnp.float32),
-            pltpu.VMEM((2, sp_count * CORES, 2, 2 * state_rows, VD), jnp.float32),
-            dma((7,)), dma((2,)), dma((2, chips, PIECES)), dma(()), dma((2, chips)),
+            dma((7,)), dma(()), dma(()), dma((2,)), dma((2, chips, PIECES)), dma(()), dma((2, chips)),
             dma(()), dma((2, chips)),
             dma(()), dma(()), dma(()), dma((tp_count,)), dma(()), dma((chips,)), dma(()), dma((2,)),
         ],
         compiler_params=pltpu.CompilerParams(
-            collective_id=0, has_side_effects=True, vmem_limit_bytes=61 * 1024 * 1024 + 800 * 1024
+            collective_id=0, has_side_effects=True, vmem_limit_bytes=61 * 1024 * 1024 + 512 * 1024
         ),
     )(
         prompt.reshape(slots, piece_rows, width),
         new_token, query_proj_matrix, key_weight, value_weight,
-        map_balance[None, :], head_gain[None, :],
-    )
+    )
+    blocks = (tuple(range(1, chips - 1)), (0, chips - 1))
     keys, values, read = pl.pallas_call(
-        store_kernel,
+        functools.partial(store_kernel, blocks),
         out_shape=[
             jax.ShapeDtypeStruct((block_rows, key_width), jnp.bfloat16),
             jax.ShapeDtypeStruct((block_rows, key_width), jnp.bfloat16),
-            jax.ShapeDtypeStruct(read.shape, jnp.float32),
+            jax.ShapeDtypeStruct((seq_count, HEADS * VD), jnp.float32),
         ],
-        in_specs=[vmem, vmem],
+        in_specs=[vmem, vmem, any_space, any_space],
         out_specs=[any_space] * 3,
-        scratch_shapes=[dma((3,))],
+        scratch_shapes=[
+            pltpu.VMEM((seq_count, HEADS * VD), jnp.float32),
+            pltpu.VMEM((1, HEADS), jnp.float32),
+            pltpu.VMEM((1, VD), jnp.float32),
+            dma((5,)),
+        ],
         compiler_params=pltpu.CompilerParams(vmem_limit_bytes=1024 * 1024),
-    )(kv, read)
+    )(kv, states, map_balance[None, :], head_gain[None, :])
     shape = (1, 1, block_rows, key_width)
     return keys.reshape(shape), values.reshape(shape), read
 

time: 66.7 us -> 56.3 us (0.84)
  Pallas kernels: 65.9 us -> 55.5 us
    pallas_call x1, Pallas kernels: 64.5 us -> 54.1 us  [fused(): pl.pallas_call(functools.partial(step_kernel, (sp_count, tp_count, seq_co...]
where the time goes in v2:
time: 56.3 us; the launch traced here: 56.2 us
  Pallas kernels  55.5 us (99%)
  between operations  0.67 us (1%)
    pallas_call x1, Pallas kernels, fused(): pl.pallas_call(functools.partial(step_kernel, (sp_count, tp_count, seq_co...  54.1 us
    pallas_call x1, Pallas kernels, fused(): pl.pallas_call(functools.partial(store_kernel, blocks), out_shape=[jax.Sh...  1.38 us

profile of v2, /device:TPU:0, one launch (start us, length us, event | category | flops | bytes accessed | tf_op | source)
XLA Modules:
  0.0 56.2 jit_solution(9520502121537475171)
XLA Ops:
  0.6 0.0 copy-start.1
  0.6 0.0 copy-start
  0.7 54.1 %shard_map.94 = (bf16[2,512,1024]{2,1,0:T(8,128)(2,1)S(1)}, f32[2,8,24,128]{3,2,1,0:T(8,128)S(1)}) custom-call(bf16[4,128,2048]{2,1,0:T(8,128)(2,1)} %bitcast.7, bf16[2,2048]{1,0:T(2,128)(2,1)} %token_hbm.1, bf16[2048,128]{1,0:T(8,128)(2,1)} %wq_hbm.1, bf16[2048,128]{1,0:T(8,128)(2,1)} %wk_hbm.1, bf16[2048,128]{1,0:T(8,128)(2,1)} %wv_hbm.1), custom_call_target="tpu_custom_call" | custom-call | tf_op jit(solution)/shard_map/pallas_call | solution.py:610
  54.8 0.0 copy-done.1
  54.8 0.0 copy-done
  54.8 1.4 %shard_map.95 = (bf16[512,1024]{1,0:T(8,128)(2,1)}, bf16[512,1024]{1,0:T(8,128)(2,1)}, f32[2,1024]{1,0:T(2,128)}) custom-call(bf16[2,512,1024]{2,1,0:T(8,128)(2,1)S(1)} %get-tuple-element.8.kv, f32[2,8,24,128]{3,2,1,0:T(8,128)S(1)} %get-tuple-element.9.finbuf, f32[1,8]{1,0:T(1,128)S(1)} %bitcast.5, f32[1,128]{1,0:T(1,128)S(1)} %bitcast.6), custom_call_target="tpu_custom_call" | custom-call | tf_op jit(solution)/shard_map/pallas_call | solution.py:640
Async XLA Ops:
  0.6 54.1 %copy-start.1 = (f32[128]{0:T(128)S(1)}, f32[128]{0:T(128)}, u32[]{:S(2)}) copy-start(f32[128]{0:T(128)} %param.13) | copy-start | bytes 1540
  0.6 54.1 %copy-start = (f32[8]{0:T(128)S(1)}, f32[8]{0:T(128)}, u32[]{:S(2)}) copy-start(f32[8]{0:T(128)} %param.12) | copy-start | bytes 100

commit v3 on v2

--- a/solution.py
+++ b/solution.py
@@ -173,9 +173,9 @@
     dims,
     prompt, token_hbm, wq_hbm, wk_hbm, wv_hbm,
     kv, finbuf,
-    xbuf, wbuf, kvbuf, wq, token, qbuf, pbuf, pstat, stbuf,
-    loc, far_send, far_recv, line_send, prim_recv, xy_send, sec_recv, sib_send, sib_recv,
-    out_send, out_recv, pk_send, pk_recv, st_send, st_recv, fin_send, fin_recv,
+    xbuf, wbuf, kvbuf, upbuf, wq, token, qbuf, pbuf, pstat, stbuf,
+    loc, far_send, far_recv, line_send, prim_recv, xy_send, sec_recv, relay_recv, sib_send, sib_recv,
+    out_send, out_recv, up_recv, pk_send, pk_recv, st_send, st_recv, fin_send, fin_recv,
 ):
     sp_count, tp_count, seq_count = dims
     _, _, depth, wide = wbuf.shape
@@ -193,6 +193,10 @@
     diag = 3 - s
     prim = (s + s // 2) % 2
     sec = 1 - prim
+    turn = s // 2
+    near = jnp.minimum(z, chips - 1 - z)
+    inside = near > 0
+    outside = jnp.logical_not(inside)
     half = depth // 2
     step = half // PIECES
     part_rows = step // 2
@@ -251,19 +255,23 @@
     def has_next(direction):
         return (z > 0) if direction < 0 else (z < chips - 1)
 
+    def to_end(direction):
+        return (z == 1) if direction < 0 else (z == chips - 2)
+
     far_prompt = remote(prompt.at[diag], xbuf.at[3], far_send, far_recv, (diag, t))
     far_prompt.start()
     for m in range(2):
         loads[m].wait()
         for direction in (-1, 1):
-            @pl.when(has_next(direction))
+            @pl.when(jnp.logical_and(has_next(direction), to_end(direction)))
+            def _(direction=direction, m=m):
+                line(direction, m, z, turn)
+
+            @pl.when(jnp.logical_and(has_next(direction), jnp.logical_not(to_end(direction))))
             def _(direction=direction, m=m):
                 for p in range(PIECES):
                     line(direction, m, z, p)
         push(wbuf.at[m, z, :, lanes], sib_send, sib_recv.at[m, z], (s, sib))
-
-    near = jnp.minimum(z, chips - 1 - z)
-    inside = near > 0
 
     def source(j):
         j = j + 1
@@ -277,7 +285,8 @@
         j = jnp.where(both, e % 2, e // 4)
         m = jnp.where(both, e // 4, (e // 2) % 2)
         p = jnp.where(both, (e // 2) % 2, e % 2)
-        return j, m, p
+        single = jnp.logical_and(outside, e < 4)
+        return j, jnp.where(single, e % 2, m), jnp.where(single, turn, p)
 
     def group(g):
         both = jnp.logical_and(inside, g < 4)
@@ -292,16 +301,41 @@
         on_left = jnp.logical_and(jnp.logical_not(from_left), z > 0)
         pl.when(on_right)(lambda: line(1, m, zz, p))
         pl.when(on_left)(lambda: line(-1, m, zz, p))
-        for h, to in enumerate((xs, ys)):
-            part = wbuf.at[m, zz, span(prim * half + p * step + h * part_rows, part_rows), lanes]
-            push(part, xy_send, sec_recv.at[m, zz], (to, t))
+        single = jnp.logical_and(outside, e < 4)
+
+        @pl.when(single)
+        def _():
+            for to in (xs, ys):
+                push(view, xy_send, sec_recv.at[m, zz], (to, t))
+
+        @pl.when(jnp.logical_not(single))
+        def _():
+            for h, to in enumerate((xs, ys)):
+                part = part_of(prim, m, zz, p, h)
+                push(part, xy_send, sec_recv.at[m, zz], (to, t))
+
         push(view, sib_send, sib_recv.at[m, zz], (s, sib))
+
+    def part_of(which, m, zz, p, h):
+        return wbuf.at[m, zz, span(which * half + p * step + h * part_rows, part_rows), lanes]
 
     def arrive_secondary(g):
         j, m = group(g)
         zz, _ = source(j)
         view = wbuf.at[m, zz, span(sec * half, half), lanes]
         got(view, sec_recv.at[m, zz])
+
+        @pl.when(jnp.logical_and(outside, g < 2))
+        def _():
+            push(part_of(sec, m, zz, 1 - turn, 0), xy_send, relay_recv.at[m], (xs, t))
+            push(part_of(sec, m, zz, turn, 1), xy_send, relay_recv.at[m], (ys, t))
+
+        push(view, sib_send, sib_recv.at[m, zz], (s, sib))
+
+    def arrive_relayed(m):
+        zz, _ = source(0)
+        view = piece_of(m, zz, 1 - turn)
+        got(view, relay_recv.at[m])
         push(view, sib_send, sib_recv.at[m, zz], (s, sib))
 
     def columns_of(zz):
@@ -404,7 +438,7 @@
                 got(wbuf.at[m, z, :, sib_lanes], sib_recv.at[m, z])
             columns = product(0, m, z, core * cols, cols)
             if before is not None:
-                send_columns(*before)
+                pl.when(inside)(lambda before=before: send_columns(*before))
             before = (m, columns)
 
     def vectors():
@@ -470,40 +504,72 @@
         results(g)
         state(g)
 
-    own_at = jnp.where(inside, 7, 4)
+    own_at = jnp.where(inside, 7, 5)
 
     def work(e, _):
         arrive(e)
 
-        @pl.when(e == 0)
-        def _():
-            send_columns(*before)
+        @pl.when(e == 2)
+        def _():
+            pl.when(inside)(lambda: send_columns(*before))
+
+            @pl.when(outside)
+            def _():
+                inner = jnp.where(z == 0, t + CORES, t - CORES)
+                for m in range(2):
+                    for i, p in enumerate((xs, ys)):
+                        remote(
+                            kvbuf.at[m, i, :, columns_of(z)], upbuf.at[m, i],
+                            out_send, up_recv, (p, inner),
+                        ).start()
+
             vectors()
 
-        @pl.when(e == 1)
+        @pl.when(e == 3)
         def _():
             for p in peers:
                 push(qbuf.at[t], pk_send, pk_recv.at[t], p)
 
         pl.when(e == own_at)(own_block)
         pl.when(e == own_at + 1)(lambda: send_state(z))
-        outside = jnp.logical_not(inside)
-        done = jnp.where(e < 9, e - 6, e - 7)
-        pl.when(outside & (e >= 6) & (e != 9))(lambda: finish(done))
-        ready = jnp.where(inside, e - 10, jnp.where(e < 8, e - 5, e - 6))
-        pl.when((ready >= 0) & (inside | ((e != 8) & (e < 11))))(lambda: arrive_secondary(ready))
+        pl.when(outside & (e == 9))(lambda: compute(2))
+        ready = jnp.where(inside, e - 10, jnp.where(e < 9, e - 6, e - 7))
+        pl.when((ready >= 0) & (inside | ((e != 9) & (e < 11))))(lambda: arrive_secondary(ready))
+        pl.when(outside & (e == 10))(lambda: arrive_relayed(0))
         return 0
 
     events = 2 * groups
-    lax.fori_loop(0, events, work, 0)
-
-    def rest(g, _):
+    lax.fori_loop(jnp.where(inside, 0, 2), events, work, 0)
+
+    @pl.when(inside)
+    def _():
+        got(upbuf, up_recv)
+        outer = jnp.where(z == 1, z - 1, z + 1)
+        for m in range(2):
+            for i, p in enumerate((xs, ys)):
+                remote(
+                    upbuf.at[m, i], kv.at[m, span(p * rows, rows), columns_of(outer)],
+                    out_send, out_recv, (s, outer * CORES + c),
+                ).start()
+
+    def rest(i, _):
+        g = jnp.where(inside, i, jnp.where(i < 2, 3 * i, jnp.where(i == 2, 1, 4)))
         finish(g)
-        pl.when(g + 2 < groups)(lambda: arrive_secondary(g + 2))
+
+        @pl.when(inside & (i + 2 < groups))
+        def _():
+            arrive_secondary(i + 2)
+
+        @pl.when(outside & (i == 0))
+        def _():
+            arrive_secondary(4)
+            results(2)
+            arrive_relayed(1)
+
         return 0
 
-    lax.fori_loop(0, jnp.where(inside, groups - 1, 0), rest, 0)
-    pl.when(jnp.logical_not(inside))(lambda: arrive_secondary(groups - 1))
+    lax.fori_loop(0, jnp.where(inside, groups - 1, groups - 2), rest, 0)
+    pl.when(outside)(lambda: arrive_secondary(groups - 1))
 
     me = s * CORES + c
     ends = (0, chips - 1)
@@ -520,11 +586,11 @@
         for p in plane_peers + cross_peers + [(s, sib)]:
             push(view, fin_send, fin_recv.at[k], p)
 
+    compute(groups - 1)
+    results(groups - 1)
+    state(groups - 1)
     join_z(0, middle)
-    compute(groups - 1)
     send_joined(0, middle)
-    state(groups - 1)
-    results(groups - 1)
     join_z(1, ends)
     send_joined(1, ends)
     others = sp_count * CORES - 1
@@ -532,23 +598,26 @@
     for k in range(2):
         got(finbuf.at[k, pl.ds(0, others), fin_rows], fin_recv.at[k])
 
+    def pieces_view(count):
+        return wbuf.at[:, 0, pl.ds(0, count * step * cols // (2 * wide)), :]
+
     others_rows = pl.ds(0, 2)
     far_prompt.wait_send()
     got(kvbuf.at[:, others_rows], out_recv)
-    gone(kvbuf.at[:, others_rows], out_send)
-    gone(wbuf.at[0, pl.ds(0, chips - 1), :, lanes], xy_send)
+    for pieces, on in ((10, inside), (8, outside)):
+        pl.when(on)(lambda pieces=pieces: gone(pieces_view(pieces), out_send))
+    for pieces, on in ((12, inside), (14, outside)):
+        pl.when(on)(lambda pieces=pieces: gone(pieces_view(pieces), xy_send))
     gone(wbuf.at[:, :, :, lanes], sib_send)
     gone(qbuf.at[pl.ds(0, tp_count - 1)], pk_send)
     gone(stbuf.at[pl.ds(0, chips - 1), :, pl.ds(0, state_rows + 1)], st_send)
     gone(finbuf.at[:, pl.ds(0, others), fin_rows], fin_send)
     for direction, count in ((-1, chips - z), (1, z + 1)):
         for n in range(1, chips):
-            @pl.when(jnp.logical_and(has_next(direction), count == n))
-            def _(direction=direction, n=n):
-                gone(
-                    wbuf.at[:, pl.ds(0, n), pl.ds(0, half), lanes],
-                    line_send.at[(direction + 1) // 2],
-                )
+            for fewer in (0, 2):
+                @pl.when(has_next(direction) & (count == n) & (to_end(direction) == (fewer > 0)))
+                def _(direction=direction, pieces=4 * n - fewer):
+                    gone(pieces_view(pieces), line_send.at[(direction + 1) // 2])
 
 
 def store_kernel(
@@ -619,15 +688,16 @@
             pltpu.VMEM((slots, piece_rows, width), jnp.bfloat16),
             pltpu.VMEM((2, chips, width, CORES * cols), jnp.bfloat16),
             pltpu.VMEM((2, slots, piece_rows, key_width), jnp.bfloat16),
+            pltpu.VMEM((2, 2, piece_rows, CORES * cols), jnp.bfloat16),
             pltpu.VMEM((width, cols), jnp.bfloat16),
             pltpu.VMEM((seq_count, width), jnp.bfloat16),
             pltpu.VMEM((tp_count, 8, cols), jnp.float32),
             pltpu.VMEM((chips, 2 * state_rows, slots * piece_rows), jnp.bfloat16),
             pltpu.VMEM((chips, 2, state_rows, VD), jnp.float32),
             pltpu.VMEM((chips, chips, 2 * state_rows, VD), jnp.float32),
-            dma((7,)), dma(()), dma(()), dma((2,)), dma((2, chips, PIECES)), dma(()), dma((2, chips)),
+            dma((7,)), dma(()), dma(()), dma((2,)), dma((2, chips, PIECES)), dma(()), dma((2, chips)), dma((2,)),
             dma(()), dma((2, chips)),
-            dma(()), dma(()), dma(()), dma((tp_count,)), dma(()), dma((chips,)), dma(()), dma((2,)),
+            dma(()), dma(()), dma(()), dma(()), dma((tp_count,)), dma(()), dma((chips,)), dma(()), dma((2,)),
         ],
         compiler_params=pltpu.CompilerParams(
             collective_id=0, has_side_effects=True, vmem_limit_bytes=61 * 1024 * 1024 + 512 * 1024

time: 56.3 us -> 54.1 us (0.961)
  Pallas kernels: 55.5 us -> 53.2 us
    pallas_call x1, Pallas kernels: 54.1 us -> 51.8 us  [fused(): pl.pallas_call(functools.partial(step_kernel, (sp_count, tp_count, seq_co...]
where the time goes in v3:
time: 54.1 us; the launch traced here: 53.9 us
  Pallas kernels  53.2 us (98%)
  between operations  0.67 us (1%)
    pallas_call x1, Pallas kernels, fused(): pl.pallas_call(functools.partial(step_kernel, (sp_count, tp_count, seq_co...  51.8 us
    pallas_call x1, Pallas kernels, fused(): pl.pallas_call(functools.partial(store_kernel, blocks), out_shape=[jax.Sh...  1.38 us

profile of v3, /device:TPU:0, one launch (start us, length us, event | category | flops | bytes accessed | tf_op | source)
XLA Modules:
  0.0 53.9 jit_solution(1897530398915512998)
XLA Ops:
  0.6 0.0 copy-start.1
  0.6 0.0 copy-start
  0.7 51.8 %shard_map.94 = (bf16[2,512,1024]{2,1,0:T(8,128)(2,1)S(1)}, f32[2,8,24,128]{3,2,1,0:T(8,128)S(1)}) custom-call(bf16[4,128,2048]{2,1,0:T(8,128)(2,1)} %bitcast.7, bf16[2,2048]{1,0:T(2,128)(2,1)} %token_hbm.1, bf16[2048,128]{1,0:T(8,128)(2,1)} %wq_hbm.1, bf16[2048,128]{1,0:T(8,128)(2,1)} %wk_hbm.1, bf16[2048,128]{1,0:T(8,128)(2,1)} %wv_hbm.1), custom_call_target="tpu_custom_call" | custom-call | tf_op jit(solution)/shard_map/pallas_call | solution.py:679
  52.5 0.0 copy-done.1
  52.5 0.0 copy-done
  52.5 1.4 %shard_map.95 = (bf16[512,1024]{1,0:T(8,128)(2,1)}, bf16[512,1024]{1,0:T(8,128)(2,1)}, f32[2,1024]{1,0:T(2,128)}) custom-call(bf16[2,512,1024]{2,1,0:T(8,128)(2,1)S(1)} %get-tuple-element.8.kv, f32[2,8,24,128]{3,2,1,0:T(8,128)S(1)} %get-tuple-element.9.finbuf, f32[1,8]{1,0:T(1,128)S(1)} %bitcast.5, f32[1,128]{1,0:T(1,128)S(1)} %bitcast.6), custom_call_target="tpu_custom_call" | custom-call | tf_op jit(solution)/shard_map/pallas_call | solution.py:710
Async XLA Ops:
  0.6 51.9 %copy-start.1 = (f32[128]{0:T(128)S(1)}, f32[128]{0:T(128)}, u32[]{:S(2)}) copy-start(f32[128]{0:T(128)} %param.13) | copy-start | bytes 1540
  0.6 51.9 %copy-start = (f32[8]{0:T(128)S(1)}, f32[8]{0:T(128)}, u32[]{:S(2)}) copy-start(f32[8]{0:T(128)} %param.12) | copy-start | bytes 100

commit v4 on v3

--- a/solution.py
+++ b/solution.py
@@ -173,7 +173,7 @@
     dims,
     prompt, token_hbm, wq_hbm, wk_hbm, wv_hbm,
     kv, finbuf,
-    xbuf, wbuf, kvbuf, upbuf, wq, token, qbuf, pbuf, pstat, stbuf,
+    xbuf, wbuf, kvbuf, upbuf, partial, wq, token, qbuf, pbuf, pstat, stbuf,
     loc, far_send, far_recv, line_send, prim_recv, xy_send, sec_recv, relay_recv, sib_send, sib_recv,
     out_send, out_recv, up_recv, pk_send, pk_recv, st_send, st_recv, fin_send, fin_recv,
 ):
@@ -218,15 +218,20 @@
     for a in loads:
         a.start()
 
-    peers = [(s, (t + d) % tp_count) for d in range(1, tp_count)]
     z_peers = [(s, (t + d * CORES) % tp_count) for d in range(1, chips)]
     plane_peers = [((s + d) % sp_count, t) for d in range(1, sp_count)]
     cross_peers = [((s + d) % sp_count, sib) for d in range(1, sp_count)]
     barrier = pltpu.get_barrier_semaphore()
-    greeted = peers + plane_peers + cross_peers
+    greeted = plane_peers + [(s, sib)]
+
+    def greet(p):
+        pl.semaphore_signal(barrier, inc=1, device_id=p, device_id_type=MESH)
+
+    pl.when(z > 0)(lambda: greet((s, t - CORES)))
+    pl.when(z < chips - 1)(lambda: greet((s, t + CORES)))
     for p in greeted:
-        pl.semaphore_signal(barrier, inc=1, device_id=p, device_id_type=MESH)
-    pl.semaphore_wait(barrier, len(greeted))
+        greet(p)
+    pl.semaphore_wait(barrier, len(greeted) + jnp.where(inside, 2, 1))
 
     def remote(src, dst, send, recv, dev):
         return pltpu.make_async_remote_copy(
@@ -272,6 +277,8 @@
                 for p in range(PIECES):
                     line(direction, m, z, p)
         push(wbuf.at[m, z, :, lanes], sib_send, sib_recv.at[m, z], (s, sib))
+    inner = jnp.where(z == 0, t + CORES, t - CORES)
+    outer = jnp.where(z == 1, z - 1, z + 1)
 
     def source(j):
         j = j + 1
@@ -308,13 +315,16 @@
             for to in (xs, ys):
                 push(view, xy_send, sec_recv.at[m, zz], (to, t))
 
-        @pl.when(jnp.logical_not(single))
+        whole = jnp.logical_and(inside, zz == outer)
+
+        @pl.when(jnp.logical_not(jnp.logical_or(single, whole)))
         def _():
             for h, to in enumerate((xs, ys)):
                 part = part_of(prim, m, zz, p, h)
                 push(part, xy_send, sec_recv.at[m, zz], (to, t))
 
-        push(view, sib_send, sib_recv.at[m, zz], (s, sib))
+        last = jnp.logical_and(j == chips - 2, m == 1)
+        push(view, sib_send, sib_recv.at[jnp.where(last, 2, m), zz], (s, sib))
 
     def part_of(which, m, zz, p, h):
         return wbuf.at[m, zz, span(which * half + p * step + h * part_rows, part_rows), lanes]
@@ -358,12 +368,41 @@
     def multiply(m, zz):
         got(wbuf.at[m, zz, :, sib_lanes], sib_recv.at[m, zz])
 
-        def some(pair, _):
+        def body(pair, _):
             product(pair, m, zz, 0, wide)
             return 0
 
-        lax.fori_loop(0, 2, some, 0)
+        lax.fori_loop(0, 2, body, 0)
         keep(m, columns_of(zz))
+
+    last_zz = source(chips - 2)[0]
+
+    def halves(pair, which):
+        at = span(which * half, half)
+        return jnp.dot(
+            xbuf[pl.ds(2 * pair, 2), :, at].reshape(-1, half), wbuf[1, last_zz, at, :],
+            preferred_element_type=jnp.float32,
+        )
+
+    def last_begin():
+        got(wbuf.at[1, last_zz, span(prim * half, half), sib_lanes], sib_recv.at[2, last_zz])
+
+        def body(pair, _):
+            partial[pair] = halves(pair, prim)
+            return 0
+
+        lax.fori_loop(0, 2, body, 0)
+
+    def last_end():
+        got(wbuf.at[1, last_zz, span(sec * half, half), sib_lanes], sib_recv.at[1, last_zz])
+
+        def body(pair, _):
+            out = (partial[pair] + halves(pair, sec)).astype(jnp.bfloat16)
+            kvbuf[1, pl.ds(2 * pair, 2), :, columns_of(last_zz)] = out.reshape(2, rows, wide)
+            return 0
+
+        lax.fori_loop(0, 2, body, 0)
+        keep(1, columns_of(last_zz))
 
     def send_columns(m, columns):
         for i, p in enumerate((xs, ys)):
@@ -428,6 +467,17 @@
         for p in z_peers:
             push(view, st_send, st_recv.at[zz], p)
 
+    def send_up(slot, m, zz, recv):
+        for i, p in enumerate((xs, ys)):
+            remote(kvbuf.at[m, i, :, columns_of(zz)], upbuf.at[slot, i], out_send, recv, (p, inner)).start()
+
+    def pass_down(slot, m, zz):
+        for i, p in enumerate((xs, ys)):
+            remote(
+                upbuf.at[slot, i], kv.at[m, span(p * rows, rows), columns_of(zz)],
+                out_send, out_recv, (s, outer * CORES + c),
+            ).start()
+
     mine_at = chips - 1
     loads[2].wait()
     loads[3].wait()
@@ -461,7 +511,6 @@
             return 0
 
         lax.fori_loop(0, 2, some, 0)
-        got(qbuf.at[sib], pk_recv.at[sib])
         score(mine_at, z)
         new = new_rows(z)
         own_score = jnp.sum(query_of(new) * by_seq(new, seq_count), axis=1, keepdims=True) * scale
@@ -480,8 +529,7 @@
 
         @pl.when(m == 0)
         def _():
-            for i in range(CORES):
-                got(qbuf.at[zz * CORES + i], pk_recv.at[zz * CORES + i])
+            got(qbuf.at[span(zz * CORES, CORES)], pk_recv.at[zz])
             score(j, zz)
 
         @pl.when(m == 1)
@@ -512,64 +560,54 @@
         @pl.when(e == 2)
         def _():
             pl.when(inside)(lambda: send_columns(*before))
+            vectors()
+
+        @pl.when(e == 3)
+        def _():
+            push(qbuf.at[t], pk_send, pk_recv.at[z], (s, sib))
+
+        @pl.when(e == 4)
+        def _():
+            got(qbuf.at[sib], pk_recv.at[z])
+            for p in z_peers:
+                push(qbuf.at[span(z * CORES, CORES)], pk_send, pk_recv.at[z], p)
 
             @pl.when(outside)
             def _():
-                inner = jnp.where(z == 0, t + CORES, t - CORES)
                 for m in range(2):
-                    for i, p in enumerate((xs, ys)):
-                        remote(
-                            kvbuf.at[m, i, :, columns_of(z)], upbuf.at[m, i],
-                            out_send, up_recv, (p, inner),
-                        ).start()
-
-            vectors()
-
-        @pl.when(e == 3)
-        def _():
-            for p in peers:
-                push(qbuf.at[t], pk_send, pk_recv.at[t], p)
+                    view = wbuf.at[m, z, span(sec * half, half), lanes]
+                    push(view, line_send.at[jnp.where(z == 0, 1, 0)], sec_recv.at[m, z], (s, inner))
+                for m in range(2):
+                    send_up(m, m, z, up_recv.at[0])
 
         pl.when(e == own_at)(own_block)
         pl.when(e == own_at + 1)(lambda: send_state(z))
-        pl.when(outside & (e == 9))(lambda: compute(2))
-        ready = jnp.where(inside, e - 10, jnp.where(e < 9, e - 6, e - 7))
-        pl.when((ready >= 0) & (inside | ((e != 9) & (e < 11))))(lambda: arrive_secondary(ready))
-        pl.when(outside & (e == 10))(lambda: arrive_relayed(0))
+        pl.when(outside & (e >= 9) & (e < 11))(lambda: arrive_relayed(e - 9))
+        pl.when(outside & (e == 9))(lambda: send_up(2, 0, source(1)[0], up_recv.at[1]))
+        ready = jnp.where(inside, e - 9, jnp.where(e < 9, e - 6, e - 7))
+        pl.when((ready >= 0) & (inside | (e != 9)))(lambda: arrive_secondary(ready))
+        now = jnp.where(inside, e - 10, jnp.where(e == 8, 2, e - 9))
+        pl.when(jnp.where(inside, e >= 10, (e >= 8) & (e < 11)))(lambda: compute(now))
         return 0
 
     events = 2 * groups
     lax.fori_loop(jnp.where(inside, 0, 2), events, work, 0)
-
-    @pl.when(inside)
-    def _():
-        got(upbuf, up_recv)
-        outer = jnp.where(z == 1, z - 1, z + 1)
-        for m in range(2):
-            for i, p in enumerate((xs, ys)):
-                remote(
-                    upbuf.at[m, i], kv.at[m, span(p * rows, rows), columns_of(outer)],
-                    out_send, out_recv, (s, outer * CORES + c),
-                ).start()
+    results(0)
+    results(1)
+    state(1)
 
     def rest(i, _):
-        g = jnp.where(inside, i, jnp.where(i < 2, 3 * i, jnp.where(i == 2, 1, 4)))
-        finish(g)
-
-        @pl.when(inside & (i + 2 < groups))
+        @pl.when(inside & (i == 2))
         def _():
-            arrive_secondary(i + 2)
-
-        @pl.when(outside & (i == 0))
-        def _():
-            arrive_secondary(4)
-            results(2)
-            arrive_relayed(1)
-
+            got(upbuf.at[pl.ds(0, 2)], up_recv.at[0])
+            for m in range(2):
+                pass_down(m, m, outer)
+
+        pl.when(inside & (i < 2))(lambda: arrive_secondary(i + 3))
+        finish(jnp.where(inside, i + 2, i + 3))
         return 0
 
-    lax.fori_loop(0, jnp.where(inside, groups - 1, groups - 2), rest, 0)
-    pl.when(outside)(lambda: arrive_secondary(groups - 1))
+    lax.fori_loop(0, jnp.where(inside, 3, 2), rest, 0)
 
     me = s * CORES + c
     ends = (0, chips - 1)
@@ -586,9 +624,18 @@
         for p in plane_peers + cross_peers + [(s, sib)]:
             push(view, fin_send, fin_recv.at[k], p)
 
-    compute(groups - 1)
+    last_begin()
+    arrive_secondary(groups - 1)
+    last_end()
+    pack(stbuf.at[z, last_zz], 0, state_rows, weigh(chips - 2, last_zz))
     results(groups - 1)
     state(groups - 1)
+
+    @pl.when(inside)
+    def _():
+        got(upbuf.at[2], up_recv.at[1])
+        pass_down(2, 0, 2 * z - outer)
+
     join_z(0, middle)
     send_joined(0, middle)
     join_z(1, ends)
@@ -604,20 +651,19 @@
     others_rows = pl.ds(0, 2)
     far_prompt.wait_send()
     got(kvbuf.at[:, others_rows], out_recv)
-    for pieces, on in ((10, inside), (8, outside)):
+    for pieces, on in ((11, inside), (8, outside)):
         pl.when(on)(lambda pieces=pieces: gone(pieces_view(pieces), out_send))
-    for pieces, on in ((12, inside), (14, outside)):
+    for pieces, on in ((8, inside), (14, outside)):
         pl.when(on)(lambda pieces=pieces: gone(pieces_view(pieces), xy_send))
     gone(wbuf.at[:, :, :, lanes], sib_send)
     gone(qbuf.at[pl.ds(0, tp_count - 1)], pk_send)
     gone(stbuf.at[pl.ds(0, chips - 1), :, pl.ds(0, state_rows + 1)], st_send)
     gone(finbuf.at[:, pl.ds(0, others), fin_rows], fin_send)
-    for direction, count in ((-1, chips - z), (1, z + 1)):
-        for n in range(1, chips):
-            for fewer in (0, 2):
-                @pl.when(has_next(direction) & (count == n) & (to_end(direction) == (fewer > 0)))
-                def _(direction=direction, pieces=4 * n - fewer):
-                    gone(pieces_view(pieces), line_send.at[(direction + 1) // 2])
+    for direction in (-1, 1):
+        for pieces, last in ((10, True), (8, False)):
+            @pl.when(jnp.logical_and(has_next(direction), to_end(direction) == last))
+            def _(direction=direction, pieces=pieces):
+                gone(pieces_view(pieces), line_send.at[(direction + 1) // 2])
 
 
 def store_kernel(
@@ -688,7 +734,8 @@
             pltpu.VMEM((slots, piece_rows, width), jnp.bfloat16),
             pltpu.VMEM((2, chips, width, CORES * cols), jnp.bfloat16),
             pltpu.VMEM((2, slots, piece_rows, key_width), jnp.bfloat16),
-            pltpu.VMEM((2, 2, piece_rows, CORES * cols), jnp.bfloat16),
+            pltpu.VMEM((3, 2, piece_rows, CORES * cols), jnp.bfloat16),
+            pltpu.VMEM((2, 2 * piece_rows, CORES * cols), jnp.float32),
             pltpu.VMEM((width, cols), jnp.bfloat16),
             pltpu.VMEM((seq_count, width), jnp.bfloat16),
             pltpu.VMEM((tp_count, 8, cols), jnp.float32),
@@ -696,8 +743,8 @@
             pltpu.VMEM((chips, 2, state_rows, VD), jnp.float32),
             pltpu.VMEM((chips, chips, 2 * state_rows, VD), jnp.float32),
             dma((7,)), dma(()), dma(()), dma((2,)), dma((2, chips, PIECES)), dma(()), dma((2, chips)), dma((2,)),
-            dma(()), dma((2, chips)),
-            dma(()), dma(()), dma(()), dma(()), dma((tp_count,)), dma(()), dma((chips,)), dma(()), dma((2,)),
+            dma(()), dma((3, chips)),
+            dma(()), dma(()), dma((2,)), dma(()), dma((chips,)), dma(()), dma((chips,)), dma(()), dma((2,)),
         ],
         compiler_params=pltpu.CompilerParams(
             collective_id=0, has_side_effects=True, vmem_limit_bytes=61 * 1024 * 1024 + 512 * 1024

time: 54.1 us -> 51.2 us (0.946)
  Pallas kernels: 53.2 us -> 50.4 us
    pallas_call x1, Pallas kernels: 51.8 us -> 49 us  [fused(): pl.pallas_call(functools.partial(step_kernel, (sp_count, tp_count, seq_co...]
where the time goes in v4:
time: 51.2 us; the launch traced here: 51 us
  Pallas kernels  50.4 us (98%)
  between operations  0.67 us (1%)
    pallas_call x1, Pallas kernels, fused(): pl.pallas_call(functools.partial(step_kernel, (sp_count, tp_count, seq_co...  49 us
    pallas_call x1, Pallas kernels, fused(): pl.pallas_call(functools.partial(store_kernel, blocks), out_shape=[jax.Sh...  1.38 us

profile of v4, /device:TPU:0, one launch (start us, length us, event | category | flops | bytes accessed | tf_op | source)
XLA Modules:
  0.0 51.0 jit_solution(15896189090054658450)
XLA Ops:
  0.6 0.0 copy-start.1
  0.6 0.0 copy-start
  0.7 49.0 %shard_map.94 = (bf16[2,512,1024]{2,1,0:T(8,128)(2,1)S(1)}, f32[2,8,24,128]{3,2,1,0:T(8,128)S(1)}) custom-call(bf16[4,128,2048]{2,1,0:T(8,128)(2,1)} %bitcast.7, bf16[2,2048]{1,0:T(2,128)(2,1)} %token_hbm.1, bf16[2048,128]{1,0:T(8,128)(2,1)} %wq_hbm.1, bf16[2048,128]{1,0:T(8,128)(2,1)} %wk_hbm.1, bf16[2048,128]{1,0:T(8,128)(2,1)} %wv_hbm.1), custom_call_target="tpu_custom_call" | custom-call | tf_op jit(solution)/shard_map/pallas_call | solution.py:725
  49.6 0.0 copy-done.1
  49.7 0.0 copy-done
  49.7 1.4 %shard_map.95 = (bf16[512,1024]{1,0:T(8,128)(2,1)}, bf16[512,1024]{1,0:T(8,128)(2,1)}, f32[2,1024]{1,0:T(2,128)}) custom-call(bf16[2,512,1024]{2,1,0:T(8,128)(2,1)S(1)} %get-tuple-element.8.kv, f32[2,8,24,128]{3,2,1,0:T(8,128)S(1)} %get-tuple-element.9.finbuf, f32[1,8]{1,0:T(1,128)S(1)} %bitcast.5, f32[1,128]{1,0:T(1,128)S(1)} %bitcast.6), custom_call_target="tpu_custom_call" | custom-call | tf_op jit(solution)/shard_map/pallas_call | solution.py:757
Async XLA Ops:
  0.6 49.0 %copy-start.1 = (f32[128]{0:T(128)S(1)}, f32[128]{0:T(128)}, u32[]{:S(2)}) copy-start(f32[128]{0:T(128)} %param.13) | copy-start | bytes 1540
  0.6 49.0 %copy-start = (f32[8]{0:T(128)S(1)}, f32[8]{0:T(128)}, u32[]{:S(2)}) copy-start(f32[8]{0:T(128)} %param.12) | copy-start | bytes 100

commit v5 on v4

--- a/solution.py
+++ b/solution.py
@@ -361,6 +361,12 @@
         kvbuf[m, at, :, columns] = out.reshape(2, rows, width)
         return columns
 
+    def whole_product(m, zz):
+        out = jnp.dot(
+            xbuf[...].reshape(-1, depth), wbuf[m, zz], preferred_element_type=jnp.float32
+        ).astype(jnp.bfloat16)
+        kvbuf[m, :, :, columns_of(zz)] = out.reshape(sp_count, rows, wide)
+
     def keep(m, columns):
         for i, slot in ((2, s), (3, diag)):
             kv[m, span(slot * rows, rows), columns] = kvbuf[m, i, :, columns]
@@ -368,40 +374,25 @@
     def multiply(m, zz):
         got(wbuf.at[m, zz, :, sib_lanes], sib_recv.at[m, zz])
 
-        def body(pair, _):
-            product(pair, m, zz, 0, wide)
-            return 0
-
-        lax.fori_loop(0, 2, body, 0)
+        whole_product(m, zz)
         keep(m, columns_of(zz))
 
     last_zz = source(chips - 2)[0]
 
-    def halves(pair, which):
+    def halves(which):
         at = span(which * half, half)
         return jnp.dot(
-            xbuf[pl.ds(2 * pair, 2), :, at].reshape(-1, half), wbuf[1, last_zz, at, :],
-            preferred_element_type=jnp.float32,
+            xbuf[:, :, at].reshape(-1, half), wbuf[1, last_zz, at, :], preferred_element_type=jnp.float32
         )
 
     def last_begin():
         got(wbuf.at[1, last_zz, span(prim * half, half), sib_lanes], sib_recv.at[2, last_zz])
-
-        def body(pair, _):
-            partial[pair] = halves(pair, prim)
-            return 0
-
-        lax.fori_loop(0, 2, body, 0)
+        partial[...] = halves(prim)
 
     def last_end():
         got(wbuf.at[1, last_zz, span(sec * half, half), sib_lanes], sib_recv.at[1, last_zz])
-
-        def body(pair, _):
-            out = (partial[pair] + halves(pair, sec)).astype(jnp.bfloat16)
-            kvbuf[1, pl.ds(2 * pair, 2), :, columns_of(last_zz)] = out.reshape(2, rows, wide)
-            return 0
-
-        lax.fori_loop(0, 2, body, 0)
+        out = (partial[...] + halves(sec)).astype(jnp.bfloat16)
+        kvbuf[1, :, :, columns_of(last_zz)] = out.reshape(sp_count, rows, wide)
         keep(1, columns_of(last_zz))
 
     def send_columns(m, columns):
@@ -587,14 +578,13 @@
         ready = jnp.where(inside, e - 9, jnp.where(e < 9, e - 6, e - 7))
         pl.when((ready >= 0) & (inside | (e != 9)))(lambda: arrive_secondary(ready))
         now = jnp.where(inside, e - 10, jnp.where(e == 8, 2, e - 9))
-        pl.when(jnp.where(inside, e >= 10, (e >= 8) & (e < 11)))(lambda: compute(now))
+        pl.when(jnp.where(inside, e >= 10, (e == 8) | (e == 9)))(lambda: compute(now))
         return 0
 
     events = 2 * groups
     lax.fori_loop(jnp.where(inside, 0, 2), events, work, 0)
     results(0)
-    results(1)
-    state(1)
+    pl.when(inside)(lambda: results(1))
 
     def rest(i, _):
         @pl.when(inside & (i == 2))
@@ -604,10 +594,16 @@
                 pass_down(m, m, outer)
 
         pl.when(inside & (i < 2))(lambda: arrive_secondary(i + 3))
-        finish(jnp.where(inside, i + 2, i + 3))
+
+        @pl.when(i == 2)
+        def _():
+            last_begin()
+            arrive_secondary(groups - 1)
+
+        finish(jnp.where(outside & (i == 0), 1, i + 2))
         return 0
 
-    lax.fori_loop(0, jnp.where(inside, 3, 2), rest, 0)
+    lax.fori_loop(0, 3, rest, 0)
 
     me = s * CORES + c
     ends = (0, chips - 1)
@@ -624,8 +620,6 @@
         for p in plane_peers + cross_peers + [(s, sib)]:
             push(view, fin_send, fin_recv.at[k], p)
 
-    last_begin()
-    arrive_secondary(groups - 1)
     last_end()
     pack(stbuf.at[z, last_zz], 0, state_rows, weigh(chips - 2, last_zz))
     results(groups - 1)
@@ -735,7 +729,7 @@
             pltpu.VMEM((2, chips, width, CORES * cols), jnp.bfloat16),
             pltpu.VMEM((2, slots, piece_rows, key_width), jnp.bfloat16),
             pltpu.VMEM((3, 2, piece_rows, CORES * cols), jnp.bfloat16),
-            pltpu.VMEM((2, 2 * piece_rows, CORES * cols), jnp.float32),
+            pltpu.VMEM((slots * piece_rows, CORES * cols), jnp.float32),
             pltpu.VMEM((width, cols), jnp.bfloat16),
             pltpu.VMEM((seq_count, width), jnp.bfloat16),
             pltpu.VMEM((tp_count, 8, cols), jnp.float32),

time: 51.2 us -> 50.7 us (level)
  Pallas kernels: 50.4 us -> 49.8 us
    pallas_call x1, Pallas kernels: 49 us -> 48.5 us  [fused(): pl.pallas_call(functools.partial(step_kernel, (sp_count, tp_count, seq_co...]
where the time goes in v5:
time: 50.7 us; the launch traced here: 50.5 us
  Pallas kernels  49.8 us (98%)
  between operations  0.67 us (1%)
    pallas_call x1, Pallas kernels, fused(): pl.pallas_call(functools.partial(step_kernel, (sp_count, tp_count, seq_co...  48.5 us
    pallas_call x1, Pallas kernels, fused(): pl.pallas_call(functools.partial(store_kernel, blocks), out_shape=[jax.Sh...  1.38 us

profile of v5, /device:TPU:0, one launch (start us, length us, event | category | flops | bytes accessed | tf_op | source)
XLA Modules:
  0.0 50.5 jit_solution(14054808374128030910)
XLA Ops:
  0.6 0.0 copy-start.1
  0.6 0.0 copy-start
  0.7 48.5 %shard_map.94 = (bf16[2,512,1024]{2,1,0:T(8,128)(2,1)S(1)}, f32[2,8,24,128]{3,2,1,0:T(8,128)S(1)}) custom-call(bf16[4,128,2048]{2,1,0:T(8,128)(2,1)} %bitcast.7, bf16[2,2048]{1,0:T(2,128)(2,1)} %token_hbm.1, bf16[2048,128]{1,0:T(8,128)(2,1)} %wq_hbm.1, bf16[2048,128]{1,0:T(8,128)(2,1)} %wk_hbm.1, bf16[2048,128]{1,0:T(8,128)(2,1)} %wv_hbm.1), custom_call_target="tpu_custom_call" | custom-call | tf_op jit(solution)/shard_map/pallas_call | solution.py:719
  49.1 0.0 copy-done.1
  49.1 0.0 copy-done
  49.1 1.4 %shard_map.95 = (bf16[512,1024]{1,0:T(8,128)(2,1)}, bf16[512,1024]{1,0:T(8,128)(2,1)}, f32[2,1024]{1,0:T(2,128)}) custom-call(bf16[2,512,1024]{2,1,0:T(8,128)(2,1)S(1)} %get-tuple-element.8.kv, f32[2,8,24,128]{3,2,1,0:T(8,128)S(1)} %get-tuple-element.9.finbuf, f32[1,8]{1,0:T(1,128)S(1)} %bitcast.5, f32[1,128]{1,0:T(1,128)S(1)} %bitcast.6), custom_call_target="tpu_custom_call" | custom-call | tf_op jit(solution)/shard_map/pallas_call | solution.py:751
Async XLA Ops:
  0.6 48.5 %copy-start.1 = (f32[128]{0:T(128)S(1)}, f32[128]{0:T(128)}, u32[]{:S(2)}) copy-start(f32[128]{0:T(128)} %param.13) | copy-start | bytes 1540
  0.6 48.5 %copy-start = (f32[8]{0:T(128)S(1)}, f32[8]{0:T(128)}, u32[]{:S(2)}) copy-start(f32[8]{0:T(128)} %param.12) | copy-start | bytes 100

commit v6 on v5

--- a/solution.py
+++ b/solution.py
@@ -420,6 +420,9 @@
             [jnp.where(row_head == i, values[:, i * VD : (i + 1) * VD], 0.0) for i in range(CORES)],
         )
 
+    def queries_of(zz):
+        return qbuf.at[span(zz * CORES, CORES), pl.ds(0, seq_count)]
+
     def new_rows(zz):
         return jnp.concatenate([qbuf[zz * CORES + i] for i in range(CORES)], axis=1)
 
@@ -520,7 +523,7 @@
 
         @pl.when(m == 0)
         def _():
-            got(qbuf.at[span(zz * CORES, CORES)], pk_recv.at[zz])
+            got(queries_of(zz), pk_recv.at[zz])
             score(j, zz)
 
         @pl.when(m == 1)
@@ -538,11 +541,6 @@
         pl.when(m == 1)(lambda: send_state(zz))
 
     groups = 2 * (chips - 1)
-    def finish(g):
-        compute(g)
-        results(g)
-        state(g)
-
     own_at = jnp.where(inside, 7, 5)
 
     def work(e, _):
@@ -561,7 +559,7 @@
         def _():
             got(qbuf.at[sib], pk_recv.at[z])
             for p in z_peers:
-                push(qbuf.at[span(z * CORES, CORES)], pk_send, pk_recv.at[z], p)
+                push(queries_of(z), pk_send, pk_recv.at[z], p)
 
             @pl.when(outside)
             def _():
@@ -572,35 +570,47 @@
                     send_up(m, m, z, up_recv.at[0])
 
         pl.when(e == own_at)(own_block)
-        pl.when(e == own_at + 1)(lambda: send_state(z))
         pl.when(outside & (e >= 9) & (e < 11))(lambda: arrive_relayed(e - 9))
         pl.when(outside & (e == 9))(lambda: send_up(2, 0, source(1)[0], up_recv.at[1]))
         ready = jnp.where(inside, e - 9, jnp.where(e < 9, e - 6, e - 7))
-        pl.when((ready >= 0) & (inside | (e != 9)))(lambda: arrive_secondary(ready))
+        pl.when((ready >= 0) & (inside | ((e != 9) & (e < 11))))(lambda: arrive_secondary(ready))
         now = jnp.where(inside, e - 10, jnp.where(e == 8, 2, e - 9))
         pl.when(jnp.where(inside, e >= 10, (e == 8) | (e == 9)))(lambda: compute(now))
         return 0
 
     events = 2 * groups
     lax.fori_loop(jnp.where(inside, 0, 2), events, work, 0)
-    results(0)
-    pl.when(inside)(lambda: results(1))
+
+    @pl.when(inside)
+    def _():
+        results(0)
+        results(1)
+
+    pl.when(outside)(lambda: send_state(z))
 
     def rest(i, _):
         @pl.when(inside & (i == 2))
         def _():
+            send_state(z)
+            state(2)
+            state(3)
             got(upbuf.at[pl.ds(0, 2)], up_recv.at[0])
             for m in range(2):
                 pass_down(m, m, outer)
 
-        pl.when(inside & (i < 2))(lambda: arrive_secondary(i + 3))
+        behind = jnp.where(inside, i + 3, groups - 2)
+        pl.when(jnp.where(inside, i < 2, i == 1))(lambda: arrive_secondary(behind))
 
         @pl.when(i == 2)
         def _():
             last_begin()
             arrive_secondary(groups - 1)
 
-        finish(jnp.where(outside & (i == 0), 1, i + 2))
+        g = jnp.where(outside & (i == 0), 1, i + 2)
+        compute(g)
+        pl.when(outside & (i == 0))(lambda: results(0))
+        results(g)
+        pl.when(outside)(lambda: state(g))
         return 0
 
     lax.fori_loop(0, 3, rest, 0)
@@ -650,7 +660,8 @@
     for pieces, on in ((8, inside), (14, outside)):
         pl.when(on)(lambda pieces=pieces: gone(pieces_view(pieces), xy_send))
     gone(wbuf.at[:, :, :, lanes], sib_send)
-    gone(qbuf.at[pl.ds(0, tp_count - 1)], pk_send)
+    query_rows = qbuf.shape[1] + len(z_peers) * CORES * seq_count
+    gone(qbuf.at[pl.ds(0, query_rows // 4), pl.ds(0, 4)], pk_send)
     gone(stbuf.at[pl.ds(0, chips - 1), :, pl.ds(0, state_rows + 1)], st_send)
     gone(finbuf.at[:, pl.ds(0, others), fin_rows], fin_send)
     for direction in (-1, 1):

time: 50.7 us -> 50.1 us (0.988)
    pallas_call x1, Pallas kernels: 48.5 us -> 47.9 us  [fused(): pl.pallas_call(functools.partial(step_kernel, (sp_count, tp_count, seq_co...]
where the time goes in v6:
time: 50.1 us; the launch traced here: 50 us
  Pallas kernels  49.3 us (98%)
  between operations  0.67 us (1%)
    pallas_call x1, Pallas kernels, fused(): pl.pallas_call(functools.partial(step_kernel, (sp_count, tp_count, seq_co...  47.9 us
    pallas_call x1, Pallas kernels, fused(): pl.pallas_call(functools.partial(store_kernel, blocks), out_shape=[jax.Sh...  1.38 us

profile of v6, /device:TPU:0, one launch (start us, length us, event | category | flops | bytes accessed | tf_op | source)
XLA Modules:
  0.0 50.0 jit_solution(3344181664784178868)
XLA Ops:
  0.6 0.0 copy-start.1
  0.6 0.0 copy-start
  0.7 47.9 %shard_map.94 = (bf16[2,512,1024]{2,1,0:T(8,128)(2,1)S(1)}, f32[2,8,24,128]{3,2,1,0:T(8,128)S(1)}) custom-call(bf16[4,128,2048]{2,1,0:T(8,128)(2,1)} %bitcast.7, bf16[2,2048]{1,0:T(2,128)(2,1)} %token_hbm.1, bf16[2048,128]{1,0:T(8,128)(2,1)} %wq_hbm.1, bf16[2048,128]{1,0:T(8,128)(2,1)} %wk_hbm.1, bf16[2048,128]{1,0:T(8,128)(2,1)} %wv_hbm.1), custom_call_target="tpu_custom_call" | custom-call | tf_op jit(solution)/shard_map/pallas_call | solution.py:730
  48.6 0.0 copy-done.1
  48.6 0.0 copy-done
  48.6 1.4 %shard_map.95 = (bf16[512,1024]{1,0:T(8,128)(2,1)}, bf16[512,1024]{1,0:T(8,128)(2,1)}, f32[2,1024]{1,0:T(2,128)}) custom-call(bf16[2,512,1024]{2,1,0:T(8,128)(2,1)S(1)} %get-tuple-element.8.kv, f32[2,8,24,128]{3,2,1,0:T(8,128)S(1)} %get-tuple-element.9.finbuf, f32[1,8]{1,0:T(1,128)S(1)} %bitcast.5, f32[1,128]{1,0:T(1,128)S(1)} %bitcast.6), custom_call_target="tpu_custom_call" | custom-call | tf_op jit(solution)/shard_map/pallas_call | solution.py:762
Async XLA Ops:
  0.6 47.9 %copy-start.1 = (f32[128]{0:T(128)S(1)}, f32[128]{0:T(128)}, u32[]{:S(2)}) copy-start(f32[128]{0:T(128)} %param.13) | copy-start | bytes 1540
  0.6 47.9 %copy-start = (f32[8]{0:T(128)S(1)}, f32[8]{0:T(128)}, u32[]{:S(2)}) copy-start(f32[8]{0:T(128)} %param.12) | copy-start | bytes 100

commit v7 on v6

--- a/solution.py
+++ b/solution.py
@@ -595,8 +595,7 @@
             state(2)
             state(3)
             got(upbuf.at[pl.ds(0, 2)], up_recv.at[0])
-            for m in range(2):
-                pass_down(m, m, outer)
+            pass_down(0, 0, outer)
 
         behind = jnp.where(inside, i + 3, groups - 2)
         pl.when(jnp.where(inside, i < 2, i == 1))(lambda: arrive_secondary(behind))
@@ -637,6 +636,7 @@
 
     @pl.when(inside)
     def _():
+        pass_down(1, 1, outer)
         got(upbuf.at[2], up_recv.at[1])
         pass_down(2, 0, 2 * z - outer)
 

time: 50.1 us -> 50.1 us (level)
  no operation moved by 1% of the time
where the time goes in v7:
time: 50.1 us; the launch traced here: 50 us
  Pallas kernels  49.3 us (98%)
  between operations  0.67 us (1%)
    pallas_call x1, Pallas kernels, fused(): pl.pallas_call(functools.partial(step_kernel, (sp_count, tp_count, seq_co...  47.9 us
    pallas_call x1, Pallas kernels, fused(): pl.pallas_call(functools.partial(store_kernel, blocks), out_shape=[jax.Sh...  1.38 us

profile of v7, /device:TPU:0, one launch (start us, length us, event | category | flops | bytes accessed | tf_op | source)
XLA Modules:
  0.0 50.0 jit_solution(3074230689309487340)
XLA Ops:
  0.6 0.0 copy-start.1
  0.6 0.0 copy-start
  0.7 47.9 %shard_map.94 = (bf16[2,512,1024]{2,1,0:T(8,128)(2,1)S(1)}, f32[2,8,24,128]{3,2,1,0:T(8,128)S(1)}) custom-call(bf16[4,128,2048]{2,1,0:T(8,128)(2,1)} %bitcast.7, bf16[2,2048]{1,0:T(2,128)(2,1)} %token_hbm.1, bf16[2048,128]{1,0:T(8,128)(2,1)} %wq_hbm.1, bf16[2048,128]{1,0:T(8,128)(2,1)} %wk_hbm.1, bf16[2048,128]{1,0:T(8,128)(2,1)} %wv_hbm.1), custom_call_target="tpu_custom_call" | custom-call | tf_op jit(solution)/shard_map/pallas_call | solution.py:730
  48.6 0.0 copy-done.1
  48.6 0.0 copy-done
  48.6 1.4 %shard_map.95 = (bf16[512,1024]{1,0:T(8,128)(2,1)}, bf16[512,1024]{1,0:T(8,128)(2,1)}, f32[2,1024]{1,0:T(2,128)}) custom-call(bf16[2,512,1024]{2,1,0:T(8,128)(2,1)S(1)} %get-tuple-element.8.kv, f32[2,8,24,128]{3,2,1,0:T(8,128)S(1)} %get-tuple-element.9.finbuf, f32[1,8]{1,0:T(1,128)S(1)} %bitcast.5, f32[1,128]{1,0:T(1,128)S(1)} %bitcast.6), custom_call_target="tpu_custom_call" | custom-call | tf_op jit(solution)/shard_map/pallas_call | solution.py:762
Async XLA Ops:
  0.6 47.9 %copy-start.1 = (f32[128]{0:T(128)S(1)}, f32[128]{0:T(128)}, u32[]{:S(2)}) copy-start(f32[128]{0:T(128)} %param.13) | copy-start | bytes 1540
  0.6 47.9 %copy-start = (f32[8]{0:T(128)S(1)}, f32[8]{0:T(128)}, u32[]{:S(2)}) copy-start(f32[8]{0:T(128)} %param.12) | copy-start | bytes 100

commit v8 on v7

--- a/solution.py
+++ b/solution.py
@@ -250,12 +250,15 @@
     def span(start, size):
         return pl.ds(pl.multiple_of(start, size), size)
 
+    def slot(zz, holder):
+        return jnp.where(zz > holder, zz - 1, zz)
+
     def piece_of(m, zz, p):
         return wbuf.at[m, zz, span(prim * half + p * step, step), lanes]
 
     def line(direction, m, zz, p):
         view = piece_of(m, zz, p)
-        push(view, line_send.at[(direction + 1) // 2], prim_recv.at[m, zz, p], (s, t + direction * CORES))
+        push(view, line_send.at[(direction + 1) // 2], prim_recv.at[m, slot(zz, z + direction), p], (s, t + direction * CORES))
 
     def has_next(direction):
         return (z > 0) if direction < 0 else (z < chips - 1)
@@ -276,7 +279,7 @@
             def _(direction=direction, m=m):
                 for p in range(PIECES):
                     line(direction, m, z, p)
-        push(wbuf.at[m, z, :, lanes], sib_send, sib_recv.at[m, z], (s, sib))
+        push(wbuf.at[m, z, :, lanes], sib_send, sib_recv.at[m * chips + z], (s, sib))
     inner = jnp.where(z == 0, t + CORES, t - CORES)
     outer = jnp.where(z == 1, z - 1, z + 1)
 
@@ -303,7 +306,7 @@
         j, m, p = event(e)
         zz, from_left = source(j)
         view = piece_of(m, zz, p)
-        got(view, prim_recv.at[m, zz, p])
+        got(view, prim_recv.at[m, slot(zz, z), p])
         on_right = jnp.logical_and(from_left, z < chips - 1)
         on_left = jnp.logical_and(jnp.logical_not(from_left), z > 0)
         pl.when(on_right)(lambda: line(1, m, zz, p))
@@ -313,7 +316,7 @@
         @pl.when(single)
         def _():
             for to in (xs, ys):
-                push(view, xy_send, sec_recv.at[m, zz], (to, t))
+                push(view, xy_send, sec_recv.at[m, slot(zz, z)], (to, t))
 
         whole = jnp.logical_and(inside, zz == outer)
 
@@ -321,10 +324,10 @@
         def _():
             for h, to in enumerate((xs, ys)):
                 part = part_of(prim, m, zz, p, h)
-                push(part, xy_send, sec_recv.at[m, zz], (to, t))
+                push(part, xy_send, sec_recv.at[m, slot(zz, z)], (to, t))
 
         last = jnp.logical_and(j == chips - 2, m == 1)
-        push(view, sib_send, sib_recv.at[jnp.where(last, 2, m), zz], (s, sib))
+        push(view, sib_send, sib_recv.at[jnp.where(last, 2 * chips, m * chips + zz)], (s, sib))
 
     def part_of(which, m, zz, p, h):
         return wbuf.at[m, zz, span(which * half + p * step + h * part_rows, part_rows), lanes]
@@ -333,20 +336,20 @@
         j, m = group(g)
         zz, _ = source(j)
         view = wbuf.at[m, zz, span(sec * half, half), lanes]
-        got(view, sec_recv.at[m, zz])
+        got(view, sec_recv.at[m, slot(zz, z)])
 
         @pl.when(jnp.logical_and(outside, g < 2))
         def _():
             push(part_of(sec, m, zz, 1 - turn, 0), xy_send, relay_recv.at[m], (xs, t))
             push(part_of(sec, m, zz, turn, 1), xy_send, relay_recv.at[m], (ys, t))
 
-        push(view, sib_send, sib_recv.at[m, zz], (s, sib))
+        push(view, sib_send, sib_recv.at[m * chips + zz], (s, sib))
 
     def arrive_relayed(m):
         zz, _ = source(0)
         view = piece_of(m, zz, 1 - turn)
         got(view, relay_recv.at[m])
-        push(view, sib_send, sib_recv.at[m, zz], (s, sib))
+        push(view, sib_send, sib_recv.at[m * chips + zz], (s, sib))
 
     def columns_of(zz):
         return pl.ds(pl.multiple_of(zz * wide, wide), wide)
@@ -372,7 +375,7 @@
             kv[m, span(slot * rows, rows), columns] = kvbuf[m, i, :, columns]
 
     def multiply(m, zz):
-        got(wbuf.at[m, zz, :, sib_lanes], sib_recv.at[m, zz])
+        got(wbuf.at[m, zz, :, sib_lanes], sib_recv.at[m * chips + zz])
 
         whole_product(m, zz)
         keep(m, columns_of(zz))
@@ -386,11 +389,11 @@
         )
 
     def last_begin():
-        got(wbuf.at[1, last_zz, span(prim * half, half), sib_lanes], sib_recv.at[2, last_zz])
+        got(wbuf.at[1, last_zz, span(prim * half, half), sib_lanes], sib_recv.at[2 * chips])
         partial[...] = halves(prim)
 
     def last_end():
-        got(wbuf.at[1, last_zz, span(sec * half, half), sib_lanes], sib_recv.at[1, last_zz])
+        got(wbuf.at[1, last_zz, span(sec * half, half), sib_lanes], sib_recv.at[chips + last_zz])
         out = (partial[...] + halves(sec)).astype(jnp.bfloat16)
         kvbuf[1, :, :, columns_of(last_zz)] = out.reshape(sp_count, rows, wide)
         keep(1, columns_of(last_zz))
@@ -479,7 +482,7 @@
     for core in (c, 1 - c):
         for m in range(2):
             if core is not c:
-                got(wbuf.at[m, z, :, sib_lanes], sib_recv.at[m, z])
+                got(wbuf.at[m, z, :, sib_lanes], sib_recv.at[m * chips + z])
             columns = product(0, m, z, core * cols, cols)
             if before is not None:
                 pl.when(inside)(lambda before=before: send_columns(*before))
@@ -565,7 +568,7 @@
             def _():
                 for m in range(2):
                     view = wbuf.at[m, z, span(sec * half, half), lanes]
-                    push(view, line_send.at[jnp.where(z == 0, 1, 0)], sec_recv.at[m, z], (s, inner))
+                    push(view, line_send.at[jnp.where(z == 0, 1, 0)], sec_recv.at[m, jnp.where(z == 0, 0, chips - 2)], (s, inner))
                 for m in range(2):
                     send_up(m, m, z, up_recv.at[0])
 
@@ -747,8 +750,8 @@
             pltpu.VMEM((chips, 2 * state_rows, slots * piece_rows), jnp.bfloat16),
             pltpu.VMEM((chips, 2, state_rows, VD), jnp.float32),
             pltpu.VMEM((chips, chips, 2 * state_rows, VD), jnp.float32),
-            dma((7,)), dma(()), dma(()), dma((2,)), dma((2, chips, PIECES)), dma(()), dma((2, chips)), dma((2,)),
-            dma(()), dma((3, chips)),
+            dma((7,)), dma(()), dma(()), dma((2,)), dma((2, chips - 1, PIECES)), dma(()), dma((2, chips - 1)), dma((2,)),
+            dma(()), dma((2 * chips + 1,)),
             dma(()), dma(()), dma((2,)), dma(()), dma((chips,)), dma(()), dma((chips,)), dma(()), dma((2,)),
         ],
         compiler_params=pltpu.CompilerParams(

time: 50.1 us -> 50 us (level)
  no operation moved by 1% of the time
where the time goes in v8:
time: 50 us; the launch traced here: 49.9 us
  Pallas kernels  49.2 us (98%)
  between operations  0.67 us (1%)
    pallas_call x1, Pallas kernels, fused(): pl.pallas_call(functools.partial(step_kernel, (sp_count, tp_count, seq_co...  47.8 us
    pallas_call x1, Pallas kernels, fused(): pl.pallas_call(functools.partial(store_kernel, blocks), out_shape=[jax.Sh...  1.38 us

profile of v8, /device:TPU:0, one launch (start us, length us, event | category | flops | bytes accessed | tf_op | source)
XLA Modules:
  0.0 49.9 jit_solution(654709178102631925)
XLA Ops:
  0.6 0.0 copy-start.1
  0.6 0.0 copy-start
  0.7 47.8 %shard_map.94 = (bf16[2,512,1024]{2,1,0:T(8,128)(2,1)S(1)}, f32[2,8,24,128]{3,2,1,0:T(8,128)S(1)}) custom-call(bf16[4,128,2048]{2,1,0:T(8,128)(2,1)} %bitcast.7, bf16[2,2048]{1,0:T(2,128)(2,1)} %token_hbm.1, bf16[2048,128]{1,0:T(8,128)(2,1)} %wq_hbm.1, bf16[2048,128]{1,0:T(8,128)(2,1)} %wk_hbm.1, bf16[2048,128]{1,0:T(8,128)(2,1)} %wv_hbm.1), custom_call_target="tpu_custom_call" | custom-call | tf_op jit(solution)/shard_map/pallas_call | solution.py:733
  48.5 0.0 copy-done.1
  48.5 0.0 copy-done
  48.5 1.4 %shard_map.95 = (bf16[512,1024]{1,0:T(8,128)(2,1)}, bf16[512,1024]{1,0:T(8,128)(2,1)}, f32[2,1024]{1,0:T(2,128)}) custom-call(bf16[2,512,1024]{2,1,0:T(8,128)(2,1)S(1)} %get-tuple-element.8.kv, f32[2,8,24,128]{3,2,1,0:T(8,128)S(1)} %get-tuple-element.9.finbuf, f32[1,8]{1,0:T(1,128)S(1)} %bitcast.5, f32[1,128]{1,0:T(1,128)S(1)} %bitcast.6), custom_call_target="tpu_custom_call" | custom-call | tf_op jit(solution)/shard_map/pallas_call | solution.py:765
Async XLA Ops:
  0.6 47.9 %copy-start.1 = (f32[128]{0:T(128)S(1)}, f32[128]{0:T(128)}, u32[]{:S(2)}) copy-start(f32[128]{0:T(128)} %param.13) | copy-start | bytes 1540
  0.6 47.9 %copy-start = (f32[8]{0:T(128)S(1)}, f32[8]{0:T(128)}, u32[]{:S(2)}) copy-start(f32[8]{0:T(128)} %param.12) | copy-start | bytes 100
